TPU v7x, 128 devices: a whole 4x4x4 slice. The times are simulated.
128 devices in a mesh: fs: 16 (over z, y), tp: 8 (over x, core).
Axes of the slice: x: 4, y: 4, z: 4, core: 2. Of those that a mesh axis runs over, the one named last changes fastest.
Arguments:
- tokens: bfloat16 [16384, 2048], P(('fs', 'tp')), may hold values from -6 to 6
- norm_gain: float32 [2048], replicated, may hold values from 0.1 to 1.9
- up_weight: float32 [2048, 8192], P('fs', 'tp'), may hold values from -0.125 to 0.125
- down_weight: float32 [8192, 2048], P('tp', 'fs'), may hold values from -0.0625 to 0.0625
Outputs:
- mlp_out: bfloat16 [16384, 2048], P(('fs', 'tp'))
All inputs are finite; a program needn't handle non-finite values.
Results may differ from a plain program's by a relative error of at most 0.0017.
Values may be sent and summed in bfloat16 or wider, within the bound.
A program may use at most 64 MiB of HBM per device.

v0:
```python
import functools

import jax
import jax.numpy as jnp
from jax import lax
from jax.experimental import pallas as pl
from jax.experimental.pallas import tpu as pltpu
from jax.sharding import PartitionSpec as P

epsilon = 1e-06
MESH = pl.DeviceIdType.MESH
VMEM_LIMIT = 66_000_000


def shards(tokens, norm_gain, up_weight, down_weight):
    values = tokens.astype(jnp.float32)
    scale = lax.rsqrt(jnp.mean(values * values, axis=-1, keepdims=True) + epsilon)
    normed = (values * scale * norm_gain).astype(jnp.bfloat16)
    grouped = lax.all_gather(normed, "tp", axis=0, tiled=True)
    up = lax.all_gather(up_weight.astype(jnp.bfloat16), "fs", axis=0, tiled=True)
    pre = jnp.dot(grouped, up, preferred_element_type=jnp.float32)
    hidden = jnp.square(jax.nn.relu(pre)).astype(jnp.bfloat16)
    down = lax.all_gather(down_weight.astype(jnp.bfloat16), "fs", axis=1, tiled=True)
    terms = jnp.dot(hidden, down, preferred_element_type=jnp.float32)
    summed = lax.psum_scatter(terms, "tp", scatter_dimension=0, tiled=True)
    return summed.astype(jnp.bfloat16)


def kernel(
    nz, ny, nx, nc, cuts,
    tok_ref, gain_ref, up_ref, down_ref, out_ref,
    tok, up, down, up_out, down_out, hidden, own, s1, r1, s2, r2,
    tok_recv, tok_send, tok_pass, up_recv, up_send, up_cross, down_recv, down_send, down_cross,
    s1_send, r1_recv, s2_send, r2_recv,
):
    chips = ny * nx
    fs, tp = lax.axis_index("fs"), lax.axis_index("tp")
    z, y = fs // ny, lax.rem(fs, ny)
    x, c = tp // nc, lax.rem(tp, nc)
    other = 1 - c
    me = y * nx + x
    part = up.shape[2]
    width = down.shape[2]
    whole = width * cuts
    outer = (z == 0) | (z == nz - 1)

    def at(zz, yy, xx, cc):
        return (zz * ny + yy, xx * nc + cc)

    def chip(step):
        place = lax.rem(me + step, chips)
        return place, place // nx, lax.rem(place, nx)

    def remote(src, dst, send, recv, to):
        return pltpu.make_async_remote_copy(
            src_ref=src, dst_ref=dst, send_sem=send, recv_sem=recv, device_id=to, device_id_type=MESH
        )

    barrier = pltpu.get_barrier_semaphore()

    def greet(to):
        pl.semaphore_signal(barrier, inc=1, device_id=to, device_id_type=MESH)

    for step in range(1, chips):
        _, yy, xx = chip(step)
        greet(at(z, yy, xx, c))
    greet(at(z, y, x, other))
    pl.when(z > 0)(lambda: greet(at(z - 1, y, x, c)))
    pl.when(z < nz - 1)(lambda: greet(at(z + 1, y, x, c)))

    mine = z * ny + y
    up[mine] = up_ref[:, pl.ds(pl.multiple_of(y * part, 128), part)].astype(jnp.bfloat16)
    for step in range(1, ny):
        yy = lax.rem(y + step, ny)
        up_out[step - 1] = up_ref[:, pl.ds(pl.multiple_of(yy * part, 128), part)].astype(jnp.bfloat16)
    pl.semaphore_wait(
        barrier, chips + (z > 0).astype(jnp.int32) + (z < nz - 1).astype(jnp.int32)
    )

    def along(buf, send, recv, slot, step):
        to = z + step
        side = (step + 1) // 2
        return remote(buf.at[slot], buf.at[slot], send.at[slot, side], recv.at[slot], at(to, y, x, c))

    def pass_on(buf, send, recv, zz, slot, wait=False):
        def go(step):
            copy = along(buf, send, recv, slot, step)
            copy.wait_send() if wait else copy.start()

        pl.when((zz <= z) & (z < nz - 1))(lambda: go(1))
        pl.when((zz >= z) & (z > 0))(lambda: go(-1))

    def arrive(buf, send, recv, slot):
        along(buf, send, recv, slot, 1).wait_recv()

    def cross(buf, dst, send, recv, step):
        yy = lax.rem(y + step, ny)
        return remote(buf.at[step - 1], dst.at[mine], send.at[step - 1], recv.at[mine], at(z, yy, x, c))

    def cross_down(step, cut):
        yy = lax.rem(y + step, ny)
        at_cut, to_cut = (step - 1) * cuts + cut, mine * cuts + cut
        return remote(
            down_out.at[at_cut], down.at[to_cut], down_cross.at[at_cut], down_recv.at[to_cut], at(z, yy, x, c)
        )

    def pass_down(slot):
        for cut in range(cuts):
            pass_on(down, down_send, down_recv, z, slot * cuts + cut)

    pass_on(up, up_send, up_recv, z, mine)
    for step in range(1, ny):
        cross(up_out, up, up_cross, up_recv, step).start()

    values = tok_ref[...].astype(jnp.float32)
    scale = lax.rsqrt(jnp.mean(values * values, axis=-1, keepdims=True) + epsilon)
    tok[c * chips + me] = (values * scale * gain_ref[...]).astype(jnp.bfloat16)
    for step in range(ny):
        yy = lax.rem(y + step, ny)
        for cut in range(cuts):
            piece = down_ref[
                pl.ds(pl.multiple_of(yy * part, 128), part), cut * width:(cut + 1) * width
            ].astype(jnp.bfloat16)
            if step == 0:
                down[mine * cuts + cut] = piece
            else:
                down_out[(step - 1) * cuts + cut] = piece

    def tok_to(step):
        _, yy, xx = chip(step)
        slot = tok.at[c * chips + me]
        return remote(slot, slot, tok_send.at[step - 1], tok_recv.at[c * chips + me], at(z, yy, xx, c))

    def tok_over(place):
        slot = tok.at[c * chips + place]
        return remote(
            slot, slot, tok_pass.at[place], tok_recv.at[c * chips + place], at(z, y, x, other)
        )

    for step in range(1, chips):
        tok_to(step).start()
    tok_over(me).start()
    pass_down(mine)
    for step in range(1, ny):
        for cut in range(cuts):
            cross_down(step, cut).start()

    def take_crossed():
        for step in range(1, ny):
            slot = z * ny + lax.rem(y + step, ny)
            for cut in range(cuts):
                arrive(down, down_send, down_recv, slot * cuts + cut)
            pass_down(slot)

    def rounds(count):
        return [(0, 0)] + [(d, s) for d in range(1, count) for s in (-1, 1)]

    for number, (distance, side) in enumerate(rounds(nz)):
        zz = z + side * distance

        @pl.when((zz >= 0) & (zz < nz))
        def _():
            for step in range(ny):
                slot = zz * ny + lax.rem(y + step, ny)
                if distance > 0 or step > 0:
                    arrive(up, up_send, up_recv, slot)
                    pass_on(up, up_send, up_recv, zz, slot)

        if number == 2:
            for step in range(1, chips):
                place, _, _ = chip(step)
                slot = tok.at[c * chips + place]
                remote(slot, slot, tok_send.at[step - 1], tok_recv.at[c * chips + place], at(z, y, x, other)).wait_recv()
                tok_over(place).start()
            pl.when(outer)(take_crossed)

    pl.when(~outer)(take_crossed)
    for place in range(chips):
        slot = tok.at[other * chips + place]
        remote(
            slot, slot, tok_pass.at[place], tok_recv.at[other * chips + place], at(z, y, x, other)
        ).wait_recv()

    rows = tok.shape[0] * tok.shape[1]
    depth = tok.shape[2]
    tile = 256

    def hide(n, carry):
        columns = pl.ds(pl.multiple_of(n * tile, tile), tile)
        pre = jnp.dot(
            tok[...].reshape(rows, depth),
            up[:, :, columns].reshape(depth, tile),
            preferred_element_type=jnp.float32,
        )
        hidden[:, columns] = jnp.square(jnp.maximum(pre, 0.0)).astype(jnp.bfloat16)
        return carry

    lax.fori_loop(0, part // tile, hide, 0)

    half = rows // nc
    shard = half // chips

    def to_core(slot):
        return remote(s1.at[slot], r1.at[slot], s1_send.at[slot], r1_recv.at[slot], at(z, y, x, other))

    def to_chip(slot, step):
        place, yy, xx = chip(step)
        return remote(
            s2.at[slot, place], r2.at[slot, step - 1], s2_send.at[slot, step - 1],
            r2_recv.at[slot, step - 1], at(z, yy, xx, c),
        )

    def blocks(number):
        turn, rest = number // (ny * cuts), lax.rem(number, ny * cuts)
        distance = (turn + 1) // 2
        zz = jnp.where(lax.rem(turn, 2) == 1, z - distance, z + distance)
        return zz, zz * ny + lax.rem(y + rest // cuts, ny), lax.rem(rest, cuts)

    def project(zz, slot):
        @pl.when(zz != z)
        def _():
            arrive(down, down_send, down_recv, slot)
            pass_on(down, down_send, down_recv, zz, slot)

        theirs = hidden[pl.ds(pl.multiple_of(other * half, half), half), :]
        s1[slot] = jnp.dot(theirs, down[slot], preferred_element_type=jnp.float32)
        to_core(slot).start()
        ours = hidden[pl.ds(pl.multiple_of(c * half, half), half), :]
        own[...] = jnp.dot(ours, down[slot], preferred_element_type=jnp.float32)
        to_core(slot).wait_recv()
        s2[slot] = (own[...] + r1[slot]).reshape(chips, shard, width)
        for hop in range(1, chips):
            to_chip(slot, hop).start()

    def take(number, carry):
        zz, slot, cut = blocks(number)
        pl.when((zz >= 0) & (zz < nz))(lambda: project(zz, slot * cuts + cut))
        return carry

    lax.fori_loop(0, (2 * nz - 1) * ny * cuts, take, 0)

    def finish(number, carry):
        zz, first, cut = blocks(number)

        @pl.when((zz >= 0) & (zz < nz))
        def _():
            slot = first * cuts + cut
            total = s2[slot, me]
            for hop in range(1, chips):
                to_chip(slot, hop).wait_recv()
                total = total + r2[slot, hop - 1]
            out_ref[:, pl.ds(pl.multiple_of(slot * width, 128), width)] = total.astype(jnp.bfloat16)
            to_core(slot).wait_send()
            for hop in range(1, chips):
                to_chip(slot, hop).wait_send()
            pass_on(down, down_send, down_recv, zz, slot, wait=True)
            pl.when(cut == 0)(lambda: pass_on(up, up_send, up_recv, zz, first, wait=True))

        return carry

    lax.fori_loop(0, (2 * nz - 1) * ny * cuts, finish, 0)

    for step in range(1, ny):
        cross(up_out, up, up_cross, up_recv, step).wait_send()
        for cut in range(cuts):
            cross_down(step, cut).wait_send()
    for step in range(1, chips):
        tok_to(step).wait_send()
    for place in range(chips):
        tok_over(place).wait_send()


def solution(mesh):
    fs, tp = mesh.shape["fs"], mesh.shape["tp"]
    ny = 1
    while (2 * ny) * (2 * ny) <= fs and fs % (2 * ny) == 0:
        ny *= 2
    nz, nc = fs // ny, 2
    nx = tp // nc
    chips, cuts = ny * nx, 2
    placed = (P(("fs", "tp"), None), P(), P("fs", "tp"), P("tp", "fs"))

    def whole(tokens, norm_gain, up_weight, down_weight):
        rows, depth = tokens.shape
        share, span = up_weight.shape
        part, width = span // ny, down_weight.shape[1] // cuts
        pieces = fs * cuts
        held = chips * nc
        half = chips * rows
        vm, dma = pltpu.VMEM, pltpu.SemaphoreType.DMA
        low, full = jnp.bfloat16, jnp.float32
        shapes = [
            ((held, rows, depth), low), ((fs, share, part), low), ((pieces, part, width), low),
            ((ny - 1, share, part), low), (((ny - 1) * cuts, part, width), low), ((held * rows, part), low),
            ((half, width), full), ((pieces, half, width), full), ((pieces, half, width), full),
            ((pieces, chips, rows, width), full), ((pieces, chips - 1, rows, width), full),
        ]
        size = 0
        for shape, kind in shapes:
            count = 4 if kind == full else 2
            for extent in shape:
                count *= extent
            size += count
        size += 4 * (up_weight.size + down_weight.size) + 4 * tokens.size
        if size > VMEM_LIMIT * 9 // 10 or part % 256 or width % 128 or tp % nc or ny < 2 or chips < 2:
            return shards(tokens, norm_gain, up_weight, down_weight)
        at_vmem = pl.BlockSpec(memory_space=pltpu.VMEM)
        return pl.pallas_call(
            functools.partial(kernel, nz, ny, nx, nc, cuts),
            out_shape=jax.ShapeDtypeStruct((rows, depth), jnp.bfloat16),
            in_specs=[at_vmem] * 4,
            out_specs=at_vmem,
            scratch_shapes=[vm(shape, kind) for shape, kind in shapes] + [
                dma((held,)), dma((chips - 1,)), dma((chips,)),
                dma((fs,)), dma((fs, 2)), dma((ny - 1,)),
                dma((pieces,)), dma((pieces, 2)), dma(((ny - 1) * cuts,)),
                dma((pieces,)), dma((pieces,)), dma((pieces, chips - 1)), dma((pieces, chips - 1)),
            ],
            compiler_params=pltpu.CompilerParams(
                collective_id=0, has_side_effects=True, vmem_limit_bytes=VMEM_LIMIT
            ),
        )(tokens, norm_gain.reshape(1, depth), up_weight, down_weight)

    return jax.shard_map(
        whole, mesh=mesh, in_specs=placed, out_specs=P(("fs", "tp"), None), check_vma=False
    )
```

profile of v0, /device:TPU:1, one launch (start us, length us, event | category | flops | bytes accessed | tf_op | source)
XLA Modules:
  0.0 231.7 jit_solution(14041995372060814346)
XLA Ops:
  6.5 0.0 all-gather.4.cloned.1.call-start
  6.5 1.2 fusion
  7.8 2.0 fusion.2
  9.8 0.0 all-gather.4.cloned.1.call-update
  9.8 0.0 all-gather.6.cloned.1.call-start
  9.9 1.8 convert_element_type.20
  11.7 0.0 all-gather.6.cloned.1.call-update
  11.7 0.0 all-gather.8.cloned.1.call-start
  11.7 1.8 convert_element_type.22
  13.5 0.0 all-gather.8.cloned.1.call-update
  13.5 0.0 reduce-scatter.2.cloned.1.call-start
  13.6 31.9 %all-gather.4.cloned.1.call-done = bf16[1024,2048]{1,0:T(8,128)(2,1)} async-done(((bf16[128,2048]{1,0:T(8,128)(2,1)}), bf16[1024,2048]{1,0:T(8,128)(2,1)}) %all-gather.4.cloned.1.call-update) | async-done | bytes 4194320 | tf_op jit(solution)/shard_map/all_gather | solution.py:19
  45.5 52.7 %all-gather.6.cloned.1.call-done = bf16[2048,1024]{1,0:T(8,128)(2,1)} async-done(((bf16[128,1024]{1,0:T(8,128)(2,1)}), bf16[2048,1024]{1,0:T(8,128)(2,1)}) %all-gather.6.cloned.1.call-update) | async-done | bytes 4194320 | tf_op jit(solution)/shard_map/all_gather | solution.py:20
  98.2 57.0 %all-gather.8.cloned.1.call-done = bf16[1024,2048]{1,0:T(8,128)(2,1)} async-done(((bf16[1024,128]{1,0:T(8,128)(2,1)}), bf16[1024,2048]{1,0:T(8,128)(2,1)}) %all-gather.8.cloned.1.call-update) | async-done | bytes 4194320 | tf_op jit(solution)/shard_map/all_gather | solution.py:23
  155.2 15.0 %fusion.3 = f32[1024,2048]{1,0:T(8,128)} fusion(bf16[1024,2048]{1,0:T(8,128)(2,1)} %all-gather.8.cloned.1.call-done, bf16[1024,2048]{1,0:T(8,128)(2,1)} %all-gather.4.cloned.1.call-done, bf16[2048,1024]{1,0:T(8,128)(2,1)} %all-gather.6.cloned.1.call-done), kind=kOutput, calls=%fused_computation.6 | convolution fusion | flops 8593080320 | bytes 20971520 | tf_op jit(solution)/shard_map/dot_general | solution.py:24
  170.2 0.0 reduce-scatter.2.cloned.1.call-update
  170.2 52.8 %reduce-scatter.2.cloned.1.call-done = f32[128,2048]{1,0:T(8,128)} async-done(((f32[1024,2048]{1,0:T(8,128)}), f32[128,2048]{1,0:T(8,128)}) %reduce-scatter.2.cloned.1.call-update) | async-done | bytes 1048592 | tf_op jit(solution)/shard_map/reduce_scatter | solution.py:25
  223.1 2.1 convert_element_type.23
  (1 shorter events, 0.0 us)
Async XLA Ops:
  6.5 39.0 %all-gather.4.cloned.1.call-start = ((), (), s32[]{:S(2)}) async-start(), calls=%async_computation.1 | async-start | bytes 4718592 | tf_op jit(solution)/shard_map/all_gather | solution.py:19
  9.8 88.4 %all-gather.6.cloned.1.call-start = ((), (), s32[]{:S(2)}) async-start(), calls=%async_computation.2 | async-start | bytes 4456448 | tf_op jit(solution)/shard_map/all_gather | solution.py:20
  11.7 143.5 %all-gather.8.cloned.1.call-start = ((), (), s32[]{:S(2)}) async-start(), calls=%async_computation.3 | async-start | bytes 4456448 | tf_op jit(solution)/shard_map/all_gather | solution.py:23
  13.5 209.5 %reduce-scatter.2.cloned.1.call-start = ((), (), s32[]{:S(2)}) async-start(), calls=%async_computation.4 | async-start | bytes 9437184 | tf_op jit(solution)/shard_map/reduce_scatter | solution.py:25
Sparse Core Ops, SparseCore 0:
  9.9 35.5 all-gather.3
  47.6 50.5 all-gather.5
  100.4 54.7 all-gather.7
  170.4 52.6 reduce-scatter.1
where the time goes:
time: 232 us
  waiting for transfers between devices  194 us (84%)
  matrix products  15 us (6%)
  between operations  13.1 us (6%)
  other arithmetic  8.9 us (4%)
    all_gather x1, waiting for transfers between devices, shards(): lax.all_gather(down_weight.astype(jnp.bfloat16), 'fs', axis=1, tiled=True)  57 us
    reduce_scatter x1, waiting for transfers between devices, shards(): summed = lax.psum_scatter(terms, 'tp', scatter_dimension=0, tiled=True)  52.8 us
    all_gather x1, waiting for transfers between devices, shards(): lax.all_gather(up_weight.astype(jnp.bfloat16), 'fs', axis=0, tiled=True)  52.7 us
    all_gather x1, waiting for transfers between devices, shards(): grouped = lax.all_gather(normed, 'tp', axis=0, tiled=True)  31.9 us
    dot_general x1, matrix products, shards(): terms = jnp.dot(hidden, down, preferred_element_type=jnp.float32)  15 us
  transfers between devices with their start and end apart: 4, of which 4 were waited for; matrix products, arithmetic and copies ran while one was open for 2% of the time, Pallas kernels for 0%

commit v1 on v0

v1 whole, which is shorter than its diff:
```python
import functools

import jax
import jax.numpy as jnp
from jax import lax
from jax.experimental import pallas as pl
from jax.experimental.pallas import tpu as pltpu
from jax.sharding import PartitionSpec as P

epsilon = 1e-06
MESH = pl.DeviceIdType.MESH
VMEM_LIMIT = 60_000_000
SIDE = 4
QUARTERS = 4
POWER = 9
PEAK = 11585.0
TINY = 1e-30


def encode(block):
    largest = jnp.max(jnp.abs(block), axis=0, keepdims=True)
    level = jnp.maximum(largest, TINY).astype(jnp.bfloat16)
    t = block * (PEAK / level.astype(jnp.float32))
    t2 = t * t
    t4 = t2 * t2
    return (t4 * t4 * t).astype(jnp.bfloat16), level


def decode(code, level):
    y = code.astype(jnp.float32)
    size = jnp.exp(jnp.log(jnp.maximum(jnp.abs(y), 1e-38)) * (1.0 / POWER)) * (level * (1.0 / PEAK))
    return jnp.where(y > 0.0, size, jnp.where(y < 0.0, -size, 0.0))


def kernel(
    tok_ref, gain_ref, up_ref, down_ref, out_ref,
    tok, up, down, acc, hidden, own, rs_out, rs_in,
    tok_send, tok_recv, up_recv, up_side, down_recv, down_side, sent, side_sent, rs_send, rs_recv,
):
    fs, tp = lax.axis_index("fs"), lax.axis_index("tp")
    z, y = fs // SIDE, lax.rem(fs, SIDE)
    x, c = tp // 2, lax.rem(tp, 2)
    other = 1 - c
    mine = fs
    rows = tok.shape[1]
    share = up.shape[3]
    piece = up.shape[4]
    width = down.shape[4]

    def ring(place, step):
        return lax.rem(place + (step + SIDE), SIDE)

    def at(dz, dy, dx):
        return (ring(z, dz) * SIDE + ring(y, dy), ring(x, dx) * 2 + c)

    sibling = (fs, x * 2 + other)

    def remote(src, dst, send, recv, to):
        return pltpu.make_async_remote_copy(
            src_ref=src, dst_ref=dst, send_sem=send, recv_sem=recv, device_id=to, device_id_type=MESH
        )

    barrier = pltpu.get_barrier_semaphore()
    peers = [at(1, 0, 0), at(-1, 0, 0), at(0, 1, 0), at(0, -1, 0), at(0, 0, 1), at(0, 0, -1), at(0, 0, 2), sibling]
    for to in peers:
        pl.semaphore_signal(barrier, inc=1, device_id=to, device_id_type=MESH)

    def block(h, ia, ib):
        dz, dy = (ia, ib) if h == 0 else (ib, ia)
        return ring(z, dz) * SIDE + ring(y, dy)

    class Gather:
        def __init__(self, number, buf, recv, side):
            self.number, self.buf, self.recv, self.side = number, buf, recv, side

        def send(self, h, ia, ib, j, axis, s):
            along_z = (axis == "a") == (h == 0)
            to = at(s, 0, 0) if along_z else at(0, s, 0)
            link = (0 if along_z else 2) + (0 if s > 0 else 1)
            ref = self.buf.at[c, block(h, ia, ib), 2 * h + j]
            remote(ref, ref, sent.at[self.number, link], self.recv.at[block(h, ia, ib), 2 * h + j], to).start()

        def wait(self, h, ia, ib, j):
            f = block(h, ia, ib)
            ref = self.buf.at[c, f, 2 * h + j]
            remote(ref, ref, sent.at[self.number, 0], self.recv.at[f, 2 * h + j], sibling).wait_recv()

        def over(self, h, ia, ib):
            f = block(h, ia, ib)
            ref = self.buf.at[c, f, pl.ds(2 * h, 2)]
            remote(ref, ref, side_sent.at[self.number], self.side.at[f, h], sibling).start()

        def wait_over(self, h, ia, ib):
            f = block(h, ia, ib)
            ref = self.buf.at[other, f, pl.ds(2 * h, 2)]
            remote(ref, ref, side_sent.at[self.number], self.side.at[f, h], sibling).wait_recv()

        def first(self):
            for turn in (0, 1):
                for h in (0, 1):
                    for s in (1, -1):
                        self.send(h, 0, 0, turn if s > 0 else 1 - turn, "a", s)
            for turn in (0, 1):
                for h in (0, 1):
                    for s in (1, -1):
                        self.send(h, 0, 0, turn if s > 0 else 1 - turn, "b", s)
            for h in (0, 1):
                self.over(h, 0, 0)

        def near(self):
            for turn in (0, 1):
                for h in (0, 1):
                    for s in (1, -1):
                        j = turn if s > 0 else 1 - turn
                        self.wait(h, -s, 0, j)
                        if turn == 0:
                            self.send(h, -s, 0, j, "a", s)
                        for side in (1, -1):
                            self.send(h, -s, 0, j, "b", side)
            for h in (0, 1):
                for s in (1, -1):
                    self.over(h, -s, 0)

        def cross(self, ia):
            for turn in (0, 1):
                for h in (0, 1):
                    for s in (1, -1):
                        j = turn if s > 0 else 1 - turn
                        self.wait(h, ia, -s, j)
                        if turn == 0:
                            self.send(h, ia, -s, j, "b", s)
            for h in (0, 1):
                for s in (1, -1):
                    self.over(h, ia, -s)

        def far(self):
            for h in (0, 1):
                for j in (0, 1):
                    self.wait(h, 2, 0, j)
                    for side in (1, -1):
                        self.send(h, 2, 0, j, "b", side)
            for h in (0, 1):
                self.over(h, 2, 0)

        def last(self, ia):
            for h in (0, 1):
                for j in (0, 1):
                    self.wait(h, ia, 2, j)
                self.over(h, ia, 2)

        def drain(self):
            count = self.buf.shape[1] - 1
            ref = self.buf.at[0, pl.ds(0, count), 0]
            for link in range(4):
                remote(ref, ref, sent.at[self.number, link], sent.at[self.number, link], sibling).wait_send()
            whole = self.buf.at[0]
            remote(whole, whole, side_sent.at[self.number], side_sent.at[self.number], sibling).wait_send()

    ups = Gather(0, up, up_recv, up_side)
    downs = Gather(1, down, down_recv, down_side)

    for q in range(QUARTERS):
        up[c, mine, q] = up_ref[:, q * piece:(q + 1) * piece].astype(jnp.bfloat16)
    pl.semaphore_wait(barrier, len(peers))
    ups.first()

    values = tok_ref[...].astype(jnp.float32)
    scale = lax.rsqrt(jnp.mean(values * values, axis=-1, keepdims=True) + epsilon)
    tok[x] = (values * scale * gain_ref[...]).astype(jnp.bfloat16)
    half = rows // 2

    def token_copy(slot, part, s, number):
        ref = tok.at[slot, pl.ds(part * half, half)]
        return remote(ref, ref, tok_send.at[number], tok_recv.at[slot, part], at(0, 0, s))

    own_copies = []
    for turn in (0, 1):
        for s in (1, -1):
            part = turn if s > 0 else 1 - turn
            own_copies.append(token_copy(x, part, s, len(own_copies)))
            own_copies[-1].start()
    for q in range(QUARTERS):
        down[c, mine, q] = down_ref[q * share * 2:(q + 1) * share * 2, :].astype(jnp.bfloat16)

    def token_wait(slot, part):
        token_copy(slot, part, 1, 0).wait_recv()

    ups.near()
    for s in (1, -1):
        part = 0 if s > 0 else 1
        slot = ring(x, -s)
        token_wait(slot, part)
        own_copies.append(token_copy(slot, part, s, len(own_copies)))
        own_copies[-1].start()
    ups.cross(0)
    ups.far()
    ups.cross(-1)
    ups.cross(1)
    ups.last(0)
    ups.cross(2)
    downs.first()

    for s in (1, -1):
        token_wait(ring(x, -s), 1 if s > 0 else 0)
    for part in (0, 1):
        token_wait(ring(x, 2), part)

    tokens = tok.shape[0] * rows

    def expand(h, places, begin, end):
        for place in places:
            ups.wait_over(h, *place)
        numbers = [block(h, *place) for place in places]

        def columns(n, carry):
            core, q = n // 2, 2 * h + lax.rem(n, 2)
            slot = core * QUARTERS + q
            left = jnp.concatenate(
                [tok[:, :, pl.ds(pl.multiple_of(f * share, share), share)].reshape(tokens, share) for f in numbers], axis=1
            )
            right = jnp.concatenate([up[core, f, q] for f in numbers], axis=0)
            pre = jnp.dot(left, right, preferred_element_type=jnp.float32)
            if not begin:
                pre = pre + acc[slot]
            if end:
                hidden[slot] = jnp.square(jnp.maximum(pre, 0.0)).astype(jnp.bfloat16)
            else:
                acc[slot] = pre
            return carry

        lax.fori_loop(0, 4, columns, 0)

    for h in (0, 1):
        expand(h, [(0, 0), (-1, 0), (1, 0), (2, 0)], True, False)
    for h in (0, 1):
        expand(h, [(0, -1), (0, 1), (-1, -1), (-1, 1)], False, False)
    for h in (0, 1):
        expand(h, [(1, -1), (1, 1), (2, -1), (2, 1)], False, False)
    for ia in (-1, 1, 2):
        ups.last(ia)
    for h in (0, 1):
        expand(h, [(0, 2), (-1, 2), (1, 2), (2, 2)], False, True)

    def spot(dz, dy):
        return ring(z, dz) * SIDE + ring(y, dy)

    hops = (1, -1, 2)

    def rs_copy(pair, number):
        return remote(
            rs_out.at[pair, number], rs_in.at[pair, number], rs_send.at[pair, number], rs_recv.at[pair, number],
            at(0, 0, hops[number]),
        )

    def project(pair, places):
        for dz, dy in places:
            downs.wait_over(0, dz, dy)
            downs.wait_over(1, dy, dz)
        numbers = [spot(*place) for place in places]
        total = None
        for core in range(2):
            for q in range(QUARTERS):
                right = jnp.concatenate([down[core, f, q] for f in numbers], axis=1)
                part = jnp.dot(hidden[core * QUARTERS + q], right, preferred_element_type=jnp.float32)
                total = part if total is None else total + part
        terms = acc.at[pair]
        terms[...] = total
        for number, hop in enumerate(hops):
            to = ring(x, hop)
            code, level = encode(terms[pl.ds(pl.multiple_of(to * rows, rows), rows), :])
            rs_out[pair, number, 0:rows] = code
            rs_out[pair, number, rows:rows + 16] = jnp.broadcast_to(level, (16, level.shape[1]))
            rs_copy(pair, number).start()
        own[pair] = terms[pl.ds(pl.multiple_of(x * rows, rows), rows), :]

    def finish(pair, places):
        total = own[pair]
        for number in range(len(hops)):
            rs_copy(pair, number).wait_recv()
            level = rs_in[pair, number, rows:rows + 16].astype(jnp.float32)[0:1]
            total = total + decode(rs_in[pair, number, 0:rows], level)
        low = total.astype(jnp.bfloat16)
        for n, place in enumerate(places):
            out_ref[:, pl.ds(pl.multiple_of(spot(*place) * width, width), width)] = low[:, n * width:(n + 1) * width]

    pairs = [
        [(0, 0), (-1, 0)], [(1, 0), (0, -1)], [(0, 1), (2, 0)], [(0, 2), (-1, -1)],
        [(-1, 1), (1, -1)], [(1, 1), (2, 1)], [(2, -1), (1, 2)], [(-1, 2), (2, 2)],
    ]
    downs.near()
    downs.cross(0)
    project(0, pairs[0])
    downs.far()
    project(1, pairs[1])
    downs.cross(-1)
    downs.cross(1)
    downs.last(0)
    project(2, pairs[2])
    project(3, pairs[3])
    downs.cross(2)
    project(4, pairs[4])
    finish(0, pairs[0])
    finish(1, pairs[1])
    for ia in (-1, 1, 2):
        downs.last(ia)
    project(5, pairs[5])
    project(6, pairs[6])
    project(7, pairs[7])
    for pair in range(2, 8):
        finish(pair, pairs[pair])

    for copy in own_copies:
        copy.wait_send()
    for pair in range(8):
        for number in range(len(hops)):
            rs_copy(pair, number).wait_send()
    ups.drain()
    downs.drain()


def solution(mesh):
    fs, tp = mesh.shape["fs"], mesh.shape["tp"]
    placed = (P(("fs", "tp"), None), P(), P("fs", "tp"), P("tp", "fs"))

    def whole(tokens, norm_gain, up_weight, down_weight):
        rows, depth = tokens.shape
        share, span = up_weight.shape
        width = down_weight.shape[1]
        piece = span // QUARTERS
        groups = tp // 2
        vm, dma = pltpu.VMEM, pltpu.SemaphoreType.DMA
        low, full = jnp.bfloat16, jnp.float32
        at_vmem = pl.BlockSpec(memory_space=pltpu.VMEM)
        pairs = fs // 2
        return pl.pallas_call(
            kernel,
            out_shape=jax.ShapeDtypeStruct((rows, depth), low),
            in_specs=[at_vmem] * 4,
            out_specs=at_vmem,
            scratch_shapes=[
                vm((groups, rows, depth), low),
                vm((2, fs, QUARTERS, share, piece), low),
                vm((2, fs, QUARTERS, piece, width), low),
                vm((2 * QUARTERS, groups * rows, piece), full),
                vm((2 * QUARTERS, groups * rows, piece), low),
                vm((pairs, rows, 2 * width), full),
                vm((pairs, 3, rows + 16, 2 * width), low),
                vm((pairs, 3, rows + 16, 2 * width), low),
                dma((6,)), dma((groups, 2)),
                dma((fs, QUARTERS)), dma((fs, 2)), dma((fs, QUARTERS)), dma((fs, 2)),
                dma((2, 4)), dma((2,)), dma((pairs, 3)), dma((pairs, 3)),
            ],
            compiler_params=pltpu.CompilerParams(
                collective_id=0, has_side_effects=True, vmem_limit_bytes=VMEM_LIMIT
            ),
        )(tokens, norm_gain.reshape(1, depth), up_weight, down_weight)

    return jax.shard_map(
        whole, mesh=mesh, in_specs=placed, out_specs=P(("fs", "tp"), None), check_vma=False
    )
```

time: 232 us -> 79.6 us (0.34)
  waiting for transfers between devices: 194 us -> 0 us
  Pallas kernels: 0 us -> 76.6 us
  matrix products: 15 us -> 0 us
  between operations: 13.1 us -> 0.01 us
  other arithmetic: 8.9 us -> 0 us
    all_gather x3 -> x0, waiting for transfers between devices: 142 us -> none  [the longest x1 57 us: shards(): lax.all_gather(down_weight.astype(jnp.bfloat16), 'fs', axis=1, tiled=True)]
    pallas_call x0 -> x1, Pallas kernels: none -> 76.6 us  [whole(): pl.pallas_call(kernel, out_shape=jax.ShapeDtypeStruct((rows, depth), low)...]
    reduce_scatter x1 -> x0, waiting for transfers between devices: 52.8 us -> none  [shards(): summed = lax.psum_scatter(terms, 'tp', scatter_dimension=0, tiled=True)]
    dot_general x1 -> x0, matrix products: 15 us -> none  [shards(): terms = jnp.dot(hidden, down, preferred_element_type=jnp.float32)]
    convert_element_type x4 -> x0, other arithmetic: 7.66 us -> none  [the longest x1 2.08 us: shards(): return summed.astype(jnp.bfloat16)]
  transfers between devices with their start and end apart: 4 -> 0, of which waited for: 4 -> 0; matrix products, arithmetic and copies ran while one was open for 2% -> 0% of each run, Pallas kernels for 0% -> 0%
where the time goes in v1:
time: 79.6 us; the launch traced here: 78.5 us
  Pallas kernels  76.6 us (96%)
  local copies, waits for them, and re-layouts  1.88 us (2%)
    pallas_call x1, Pallas kernels, whole(): pl.pallas_call(kernel, out_shape=jax.ShapeDtypeStruct((rows, depth), low)...  76.6 us
    unnamed x1, local copies, waits for them, and re-layouts  1.88 us

profile of v1, /device:TPU:1, one launch (start us, length us, event | category | flops | bytes accessed | tf_op | source)
XLA Modules:
  0.0 78.5 jit_solution(10975835103643590899)
XLA Ops:
  0.0 76.6 %shard_map.46 = bf16[128,2048]{1,0:T(8,128)(2,1)} custom-call(bf16[128,2048]{1,0:T(8,128)(2,1)} %tok_ref.1, f32[1,2048]{1,0:T(1,128)} %bitcast.1, f32[128,1024]{1,0:T(8,128)} %up_ref.1, f32[1024,128]{1,0:T(8,128)} %down_ref.1), custom_call_target="tpu_custom_call" | custom-call | tf_op jit(solution)/shard_map/pallas_call | solution.py:335
  76.6 1.9 %copy.6 = bf16[128,2048]{1,0:T(8,128)(2,1)} copy(bf16[128,2048]{1,0:T(8,128)(2,1)} %shard_map.46) | data formatting | bytes 1048576

commit v2 on v1

v2 whole, which is shorter than its diff:
```python
import functools

import jax
import jax.numpy as jnp
from jax import lax
from jax.experimental import pallas as pl
from jax.experimental.pallas import tpu as pltpu
from jax.sharding import PartitionSpec as P

epsilon = 1e-06
MESH = pl.DeviceIdType.MESH
VMEM_LIMIT = 60_000_000
SIDE = 4
QUARTERS = 4
LANES = 128
POWER = 9
PEAK = 11585.0
TINY = 1e-30


def encode(block):
    largest = jnp.max(jnp.abs(block), axis=0, keepdims=True)
    level = largest[:, :LANES]
    for start in range(LANES, block.shape[1], LANES):
        level = jnp.maximum(level, largest[:, start:start + LANES])
    level = jnp.maximum(level, TINY).astype(jnp.bfloat16)
    factor = PEAK / level.astype(jnp.float32)
    codes = []
    for start in range(0, block.shape[1], LANES):
        t = block[:, start:start + LANES] * factor
        t2 = t * t
        t4 = t2 * t2
        codes.append((t4 * t4 * t).astype(jnp.bfloat16))
    return codes, jnp.broadcast_to(level, (16, LANES))


def decode(code, level):
    y = code.astype(jnp.float32)
    size = jnp.exp(jnp.log(jnp.maximum(jnp.abs(y), 1e-38)) * (1.0 / POWER)) * (level * (1.0 / PEAK))
    return jnp.where(y > 0.0, size, jnp.where(y < 0.0, -size, 0.0))


def kernel(
    tok_hbm, gain_hbm, up_hbm, down_hbm, out_ref,
    tok_ref, gain_ref, up_ref, down_ref, tok, up, down, acc, hidden, one_out, one_in, two_out, two_in,
    load, tok_send, tok_recv, arrived, crossed, sent, side_sent, one_send, one_recv, two_send, two_recv,
):
    fs, tp = lax.axis_index("fs"), lax.axis_index("tp")
    z, y = fs // SIDE, lax.rem(fs, SIDE)
    x, c = tp // 2, lax.rem(tp, 2)
    other = 1 - c
    mine = fs
    rows = tok.shape[1]
    share = up.shape[3]
    piece = up.shape[4]
    width = down.shape[4]

    def ring(place, step):
        return lax.rem(place + (step + SIDE), SIDE)

    def at(dz, dy, dx):
        return (ring(z, dz) * SIDE + ring(y, dy), ring(x, dx) * 2 + c)

    sibling = (fs, x * 2 + other)

    def remote(src, dst, send, recv, to):
        return pltpu.make_async_remote_copy(
            src_ref=src, dst_ref=dst, send_sem=send, recv_sem=recv, device_id=to, device_id_type=MESH
        )

    barrier = pltpu.get_barrier_semaphore()
    peers = [at(1, 0, 0), at(-1, 0, 0), at(0, 1, 0), at(0, -1, 0), at(0, 0, 1), at(0, 0, -1), sibling]
    for to in peers:
        pl.semaphore_signal(barrier, inc=1, device_id=to, device_id_type=MESH)

    loads = [
        pltpu.make_async_copy(src, dst, load.at[n])
        for n, (src, dst) in enumerate([(up_hbm, up_ref), (tok_hbm, tok_ref), (gain_hbm, gain_ref), (down_hbm, down_ref)])
    ]
    for copy in loads:
        copy.start()

    def block(h, ia, ib):
        dz, dy = (ia, ib) if h == 0 else (ib, ia)
        return ring(z, dz) * SIDE + ring(y, dy)

    NEAR, CROSS, FAR, LAST = 0, 2, 10, 11
    spot_of = {0: 0, -1: 1, 1: 2, 2: 3}

    class Gather:
        def __init__(self, number, buf):
            self.number, self.buf = number, buf

        def send(self, h, ia, ib, j, axis, s, group):
            along_z = (axis == "a") == (h == 0)
            to = at(s, 0, 0) if along_z else at(0, s, 0)
            ref = self.buf.at[c, block(h, ia, ib), 2 * h + j]
            remote(ref, ref, sent.at[self.number], arrived.at[self.number, group], to).start()

        def wait(self, group):
            ref = self.buf.at[c, pl.ds(0, 4), 0]
            remote(ref, ref, sent.at[self.number], arrived.at[self.number, group], sibling).wait_recv()

        def over(self, places, event):
            for h in (0, 1):
                for ia, ib in places:
                    ref = self.buf.at[c, block(h, ia, ib), pl.ds(2 * h, 2)]
                    remote(ref, ref, side_sent.at[self.number], crossed.at[self.number, event], sibling).start()

        def wait_over(self, event):
            count = 2 if event in (0, 2, 7, 8, 9, 10) else 4
            ref = self.buf.at[other, pl.ds(0, count), pl.ds(0, 2)]
            remote(ref, ref, side_sent.at[self.number], crossed.at[self.number, event], sibling).wait_recv()

        def first(self):
            for axis in ("a", "b"):
                for turn in (0, 1):
                    for h in (0, 1):
                        for s in (1, -1):
                            j = turn if s > 0 else 1 - turn
                            self.send(h, 0, 0, j, axis, s, (NEAR if axis == "a" else CROSS) + turn)
            self.over([(0, 0)], 0)

        def out(self, h, ia, j):
            for s in (1, -1):
                turn = j if s > 0 else 1 - j
                self.send(h, ia, 0, j, "b", s, CROSS + 2 * spot_of[ia] + turn)

        def near(self):
            for turn in (0, 1):
                self.wait(NEAR + turn)
                if turn == 0:
                    for h in (0, 1):
                        for s in (1, -1):
                            self.send(h, -s, 0, 0 if s > 0 else 1, "a", s, FAR)
                for h in (0, 1):
                    for s in (1, -1):
                        self.out(h, -s, turn if s > 0 else 1 - turn)
            self.over([(-1, 0), (1, 0)], 1)

        def cross(self, ia):
            for turn in (0, 1):
                self.wait(CROSS + 2 * spot_of[ia] + turn)
                if turn == 0:
                    for h in (0, 1):
                        for s in (1, -1):
                            self.send(h, ia, -s, 0 if s > 0 else 1, "b", s, LAST + spot_of[ia])
            self.over([(ia, -1), (ia, 1)], 3 + spot_of[ia])

        def far(self):
            self.wait(FAR)
            for j in (0, 1):
                for h in (0, 1):
                    self.out(h, 2, j)
            self.over([(2, 0)], 2)

        def last(self, ia):
            self.wait(LAST + spot_of[ia])
            self.over([(ia, 2)], 7 + spot_of[ia])

        def drain(self):
            ref = self.buf.at[0, pl.ds(0, self.buf.shape[1] - 1)]
            remote(ref, ref, sent.at[self.number], sent.at[self.number], sibling).wait_send()
            whole = self.buf.at[0]
            remote(whole, whole, side_sent.at[self.number], side_sent.at[self.number], sibling).wait_send()

    ups = Gather(0, up)
    downs = Gather(1, down)

    loads[0].wait()
    for q in range(QUARTERS):
        up[c, mine, q] = up_ref[:, q * piece:(q + 1) * piece].astype(jnp.bfloat16)
    pl.semaphore_wait(barrier, len(peers))
    ups.first()

    loads[1].wait()
    loads[2].wait()
    values = tok_ref[...].astype(jnp.float32)
    scale = lax.rsqrt(jnp.mean(values * values, axis=-1, keepdims=True) + epsilon)
    tok[x] = (values * scale * gain_ref[...]).astype(jnp.bfloat16)
    half = rows // 2

    def token_send(slot, part, s, group):
        ref = tok.at[slot, pl.ds(part * half, half)]
        remote(ref, ref, tok_send, tok_recv.at[group], at(0, 0, s)).start()

    def token_wait(group):
        ref = tok.at[0]
        remote(ref, ref, tok_send, tok_recv.at[group], sibling).wait_recv()

    for turn in (0, 1):
        for s in (1, -1):
            token_send(x, turn if s > 0 else 1 - turn, s, turn)
    loads[3].wait()
    for q in range(QUARTERS):
        down[c, mine, q] = down_ref[q * piece:(q + 1) * piece, :].astype(jnp.bfloat16)

    relative = (0, 1, -1, 2)

    def expand(places, begin, end, first_row, last_row):
        for h in (0, 1):
            numbers = [block(h, *place) for place in places]
            left = jnp.concatenate([
                jnp.concatenate(
                    [tok[ring(x, relative[r]), :, pl.ds(pl.multiple_of(f * share, share), share)] for f in numbers], axis=1
                ) for r in range(first_row, last_row)
            ], axis=0)
            span = slice(first_row * rows, last_row * rows)
            for core in (0, 1):
                slots = [core * QUARTERS + 2 * h + j for j in (0, 1)]
                right = jnp.concatenate([
                    jnp.concatenate([up[core, f, 2 * h + j] for f in numbers], axis=0) for j in (0, 1)
                ], axis=1)
                pre = jnp.dot(left, right, preferred_element_type=jnp.float32)
                for j, slot in enumerate(slots):
                    new = pre[:, j * piece:(j + 1) * piece]
                    if not begin:
                        new = new + acc[slot, span]
                    if end:
                        hidden[slot, span] = jnp.square(jnp.maximum(new, 0.0)).astype(jnp.bfloat16)
                    else:
                        acc[slot, span] = new

    groups = [
        [(0, 0), (-1, 0), (1, 0), (2, 0)], [(0, -1), (0, 1), (-1, -1), (-1, 1)],
        [(1, -1), (1, 1), (2, -1), (2, 1)], [(0, 2), (-1, 2), (1, 2), (2, 2)],
    ]

    ups.near()
    ups.cross(0)
    ups.far()
    token_wait(0)
    for s in (1, -1):
        token_send(ring(x, -s), 0 if s > 0 else 1, s, 2)
    ups.cross(-1)
    ups.cross(1)
    token_wait(1)
    for event in (0, 1, 2):
        ups.wait_over(event)
    expand(groups[0], True, False, 0, 3)
    ups.last(0)
    for event in (3, 4):
        ups.wait_over(event)
    expand(groups[1], False, False, 0, 3)
    ups.cross(2)
    downs.first()
    token_wait(2)
    expand(groups[0], True, False, 3, 4)
    expand(groups[1], False, False, 3, 4)
    ups.last(-1)
    for event in (5, 6):
        ups.wait_over(event)
    expand(groups[2], False, False, 0, 4)
    ups.last(1)
    ups.last(2)
    for event in (7, 8, 9, 10):
        ups.wait_over(event)
    expand(groups[3], False, True, 0, 4)

    def spot(dz, dy):
        return ring(z, dz) * SIDE + ring(y, dy)

    def one_copy(pair, way):
        return remote(
            one_out.at[pair, way], one_in.at[pair, way], one_send, one_recv.at[pair], at(0, 0, 1 - 2 * way)
        )

    def two_copy(pair, way):
        return remote(
            two_out.at[pair, way], two_in.at[pair, way], two_send, two_recv.at[pair], at(0, 0, 1 - 2 * way)
        )

    def project(pair):
        numbers = [spot(*place) for place in pairs[pair]]
        left = jnp.concatenate([hidden[slot] for slot in range(2 * QUARTERS)], axis=1)
        right = jnp.concatenate([
            jnp.concatenate([down[core, f, q] for f in numbers], axis=1) for core in (0, 1) for q in range(QUARTERS)
        ], axis=0)
        acc[pair] = jnp.dot(left, right, preferred_element_type=jnp.float32)
        for way in (0, 1):
            (code,), level = encode(acc[pair, 3 * rows:, way * width:(way + 1) * width])
            one_out[pair, way, 0:rows] = code
            one_out[pair, way, rows:rows + 16] = level
            one_copy(pair, way).start()

    def relay(pair):
        ref = one_in.at[pair]
        remote(ref, ref, one_send, one_recv.at[pair], sibling).wait_recv()
        for way in (0, 1):
            level = one_in[pair, way, rows:rows + 16].astype(jnp.float32)[0:1]
            taken = decode(one_in[pair, way, 0:rows], level)
            halves = [acc[pair, (1 + way) * rows:(2 + way) * rows, n * width:(n + 1) * width] for n in (0, 1)]
            halves[way] = halves[way] + taken
            codes, level = encode(jnp.concatenate(halves, axis=1))
            for n in (0, 1):
                two_out[pair, way, n * rows:(n + 1) * rows] = codes[n]
            two_out[pair, way, 2 * rows:2 * rows + 16] = level
            two_copy(pair, way).start()

    def finish(pair):
        ref = two_in.at[pair]
        remote(ref, ref, two_send, two_recv.at[pair], sibling).wait_recv()
        levels = [two_in[pair, way, 2 * rows:2 * rows + 16].astype(jnp.float32)[0:1] for way in (0, 1)]
        for n, place in enumerate(pairs[pair]):
            total = acc[pair, 0:rows, n * width:(n + 1) * width]
            for way in (0, 1):
                total = total + decode(two_in[pair, way, n * rows:(n + 1) * rows], levels[way])
            out_ref[:, pl.ds(pl.multiple_of(spot(*place) * width, width), width)] = total.astype(jnp.bfloat16)

    pairs = [
        [(0, 0), (-1, 0)], [(1, 0), (0, -1)], [(0, 1), (2, 0)], [(0, 2), (-1, -1)],
        [(-1, 1), (1, -1)], [(1, 1), (2, 1)], [(2, -1), (1, 2)], [(-1, 2), (2, 2)],
    ]
    downs.near()
    downs.cross(0)
    for event in (0, 1, 3):
        downs.wait_over(event)
    project(0)
    downs.far()
    project(1)
    downs.cross(-1)
    relay(0)
    downs.cross(1)
    downs.last(0)
    relay(1)
    for event in (2, 4, 5, 7):
        downs.wait_over(event)
    project(2)
    downs.cross(2)
    project(3)
    relay(2)
    project(4)
    relay(3)
    finish(0)
    finish(1)
    relay(4)
    finish(2)
    for ia in (-1, 1, 2):
        downs.last(ia)
    for event in (6, 8, 9, 10):
        downs.wait_over(event)
    project(5)
    project(6)
    relay(5)
    project(7)
    relay(6)
    finish(3)
    relay(7)
    finish(4)
    finish(5)
    finish(6)
    finish(7)

    ref = tok.at[pl.ds(0, 3)]
    remote(ref, ref, tok_send, tok_send, sibling).wait_send()
    remote(one_out, one_out, one_send, one_send, sibling).wait_send()
    remote(two_out, two_out, two_send, two_send, sibling).wait_send()
    ups.drain()
    downs.drain()


def solution(mesh):
    fs, tp = mesh.shape["fs"], mesh.shape["tp"]
    placed = (P(("fs", "tp"), None), P(), P("fs", "tp"), P("tp", "fs"))

    def whole(tokens, norm_gain, up_weight, down_weight):
        rows, depth = tokens.shape
        share, span = up_weight.shape
        width = down_weight.shape[1]
        piece = span // QUARTERS
        groups = tp // 2
        vm, dma = pltpu.VMEM, pltpu.SemaphoreType.DMA
        low, full = jnp.bfloat16, jnp.float32
        pairs = fs // 2
        return pl.pallas_call(
            kernel,
            out_shape=jax.ShapeDtypeStruct((rows, depth), low),
            in_specs=[pl.BlockSpec(memory_space=pltpu.HBM)] * 4,
            out_specs=pl.BlockSpec(memory_space=pltpu.VMEM),
            scratch_shapes=[
                vm((rows, depth), low),
                vm((1, depth), full),
                vm((share, span), full),
                vm((span, width), full),
                vm((groups, rows, depth), low),
                vm((2, fs, QUARTERS, share, piece), low),
                vm((2, fs, QUARTERS, piece, width), low),
                vm((2 * QUARTERS, groups * rows, piece), full),
                vm((2 * QUARTERS, groups * rows, piece), low),
                vm((pairs, 2, rows + 16, LANES), low),
                vm((pairs, 2, rows + 16, LANES), low),
                vm((pairs, 2, 2 * rows + 16, LANES), low),
                vm((pairs, 2, 2 * rows + 16, LANES), low),
                dma((4,)), dma, dma((3,)),
                dma((2, 15)), dma((2, 11)), dma((2,)), dma((2,)), dma, dma((pairs,)), dma, dma((pairs,)),
            ],
            compiler_params=pltpu.CompilerParams(
                collective_id=0, has_side_effects=True, vmem_limit_bytes=VMEM_LIMIT
            ),
        )(tokens, norm_gain.reshape(1, depth), up_weight, down_weight)

    return jax.shard_map(
        whole, mesh=mesh, in_specs=placed, out_specs=P(("fs", "tp"), None), check_vma=False
    )
```

time: 79.6 us -> 76 us (0.955); the launches traced: 78.5 us -> 75.8 us
  Pallas kernels: 76.6 us -> 74 us
    pallas_call x1, Pallas kernels: 76.6 us -> 74 us  [whole(): pl.pallas_call(kernel, out_shape=jax.ShapeDtypeStruct((rows, depth), low)...]
where the time goes in v2:
time: 76 us; the launch traced here: 75.8 us
  Pallas kernels  74 us (97%)
  local copies, waits for them, and re-layouts  1.88 us (2%)
    pallas_call x1, Pallas kernels, whole(): pl.pallas_call(kernel, out_shape=jax.ShapeDtypeStruct((rows, depth), low)...  74 us
    unnamed x1, local copies, waits for them, and re-layouts  1.88 us

profile of v2, /device:TPU:1, one launch (start us, length us, event | category | flops | bytes accessed | tf_op | source)
XLA Modules:
  0.0 75.8 jit_solution(10126798859982345158)
XLA Ops:
  0.0 74.0 %shard_map.46 = bf16[128,2048]{1,0:T(8,128)(2,1)} custom-call(bf16[128,2048]{1,0:T(8,128)(2,1)} %tok_hbm.1, f32[1,2048]{1,0:T(1,128)} %bitcast.1, f32[128,1024]{1,0:T(8,128)} %up_hbm.1, f32[1024,128]{1,0:T(8,128)} %down_hbm.1), custom_call_target="tpu_custom_call" | custom-call | tf_op jit(solution)/shard_map/pallas_call | solution.py:375
  74.0 1.9 %copy.6 = bf16[128,2048]{1,0:T(8,128)(2,1)} copy(bf16[128,2048]{1,0:T(8,128)(2,1)} %shard_map.46) | data formatting | bytes 1048576

commit v3 on v2

--- a/solution.py
+++ b/solution.py
@@ -84,8 +84,8 @@
         dz, dy = (ia, ib) if h == 0 else (ib, ia)
         return ring(z, dz) * SIDE + ring(y, dy)
 
-    NEAR, CROSS, FAR, LAST = 0, 2, 10, 11
-    spot_of = {0: 0, -1: 1, 1: 2, 2: 3}
+    ways = (1, -1)
+    NEAR, OWN, FAR, BACK, WIDE, EDGE, CROSS, END = 0, 2, 4, 5, 6, 8, 10, 12
 
     class Gather:
         def __init__(self, number, buf):
@@ -97,8 +97,8 @@
             ref = self.buf.at[c, block(h, ia, ib), 2 * h + j]
             remote(ref, ref, sent.at[self.number], arrived.at[self.number, group], to).start()
 
-        def wait(self, group):
-            ref = self.buf.at[c, pl.ds(0, 4), 0]
+        def wait(self, group, count=4):
+            ref = self.buf.at[c, pl.ds(0, count), 0]
             remote(ref, ref, sent.at[self.number], arrived.at[self.number, group], sibling).wait_recv()
 
         def over(self, places, event):
@@ -107,56 +107,79 @@
                     ref = self.buf.at[c, block(h, ia, ib), pl.ds(2 * h, 2)]
                     remote(ref, ref, side_sent.at[self.number], crossed.at[self.number, event], sibling).start()
 
-        def wait_over(self, event):
-            count = 2 if event in (0, 2, 7, 8, 9, 10) else 4
-            ref = self.buf.at[other, pl.ds(0, count), pl.ds(0, 2)]
-            remote(ref, ref, side_sent.at[self.number], crossed.at[self.number, event], sibling).wait_recv()
+        def wait_over(self, *events):
+            for event in events:
+                ref = self.buf.at[other, pl.ds(0, (2, 4, 4, 2, 2, 8, 4, 4, 2)[event]), pl.ds(0, 2)]
+                remote(ref, ref, side_sent.at[self.number], crossed.at[self.number, event], sibling).wait_recv()
 
         def first(self):
-            for axis in ("a", "b"):
+            for axis, group in (("a", NEAR), ("b", OWN)):
                 for turn in (0, 1):
                     for h in (0, 1):
-                        for s in (1, -1):
-                            j = turn if s > 0 else 1 - turn
-                            self.send(h, 0, 0, j, axis, s, (NEAR if axis == "a" else CROSS) + turn)
+                        for s in ways:
+                            self.send(h, 0, 0, turn if s > 0 else 1 - turn, axis, s, group + turn)
             self.over([(0, 0)], 0)
 
-        def out(self, h, ia, j):
-            for s in (1, -1):
-                turn = j if s > 0 else 1 - j
-                self.send(h, ia, 0, j, "b", s, CROSS + 2 * spot_of[ia] + turn)
+        def out(self, turn):
+            for h in (0, 1):
+                for ia in (-1, 1):
+                    for s in ways:
+                        self.send(h, ia, 0, turn if ia < 0 else 1 - turn, "b", s, WIDE + turn)
 
         def near(self):
-            for turn in (0, 1):
-                self.wait(NEAR + turn)
-                if turn == 0:
-                    for h in (0, 1):
-                        for s in (1, -1):
-                            self.send(h, -s, 0, 0 if s > 0 else 1, "a", s, FAR)
-                for h in (0, 1):
-                    for s in (1, -1):
-                        self.out(h, -s, turn if s > 0 else 1 - turn)
+            self.wait(NEAR)
+            for h in (0, 1):
+                for s in ways:
+                    self.send(h, -s, 0, 0 if s > 0 else 1, "a", s, FAR)
+            self.out(0)
+            self.wait(NEAR + 1)
             self.over([(-1, 0), (1, 0)], 1)
 
-        def cross(self, ia):
-            for turn in (0, 1):
-                self.wait(CROSS + 2 * spot_of[ia] + turn)
-                if turn == 0:
-                    for h in (0, 1):
-                        for s in (1, -1):
-                            self.send(h, ia, -s, 0 if s > 0 else 1, "b", s, LAST + spot_of[ia])
-            self.over([(ia, -1), (ia, 1)], 3 + spot_of[ia])
+        def own(self):
+            self.wait(OWN)
+            for h in (0, 1):
+                for s in ways:
+                    self.send(h, 0, -s, 0 if s > 0 else 1, "b", s, BACK)
+            self.out(1)
+            self.wait(OWN + 1)
+            self.over([(0, -1), (0, 1)], 2)
 
         def far(self):
             self.wait(FAR)
-            for j in (0, 1):
+            for turn in (0, 1):
                 for h in (0, 1):
-                    self.out(h, 2, j)
-            self.over([(2, 0)], 2)
-
-        def last(self, ia):
-            self.wait(LAST + spot_of[ia])
-            self.over([(ia, 2)], 7 + spot_of[ia])
+                    for s in ways:
+                        self.send(h, 2, 0, turn if s > 0 else 1 - turn, "b", s, CROSS + turn)
+            self.over([(2, 0)], 3)
+
+        def back(self):
+            self.wait(BACK)
+            self.over([(0, 2)], 4)
+
+        def wide(self, turn):
+            self.wait(WIDE + turn, 8)
+            for h in (0, 1):
+                for s in ways:
+                    self.send(h, -s if turn == 0 else s, -s, 0 if s > 0 else 1, "b", s, EDGE + turn)
+            if turn == 1:
+                self.over([(-1, -1), (-1, 1), (1, -1), (1, 1)], 5)
+
+        def cross(self):
+            self.wait(CROSS)
+            for h in (0, 1):
+                for s in ways:
+                    self.send(h, 2, -s, 0 if s > 0 else 1, "b", s, END)
+            self.wait(CROSS + 1)
+            self.over([(2, -1), (2, 1)], 6)
+
+        def edge(self):
+            self.wait(EDGE)
+            self.wait(EDGE + 1)
+            self.over([(-1, 2), (1, 2)], 7)
+
+        def end(self):
+            self.wait(END)
+            self.over([(2, 2)], 8)
 
         def drain(self):
             ref = self.buf.at[0, pl.ds(0, self.buf.shape[1] - 1)]
@@ -222,139 +245,166 @@
                         acc[slot, span] = new
 
     groups = [
-        [(0, 0), (-1, 0), (1, 0), (2, 0)], [(0, -1), (0, 1), (-1, -1), (-1, 1)],
-        [(1, -1), (1, 1), (2, -1), (2, 1)], [(0, 2), (-1, 2), (1, 2), (2, 2)],
+        [(0, 0), (-1, 0), (1, 0), (2, 0)], [(0, -1), (0, 1), (0, 2)], [(-1, -1), (-1, 1), (1, -1), (1, 1)],
+        [(2, -1), (2, 1)], [(-1, 2), (1, 2), (2, 2)],
     ]
 
     ups.near()
-    ups.cross(0)
+    ups.own()
     ups.far()
     token_wait(0)
-    for s in (1, -1):
+    for s in ways:
         token_send(ring(x, -s), 0 if s > 0 else 1, s, 2)
-    ups.cross(-1)
-    ups.cross(1)
+    ups.wide(0)
+    ups.back()
     token_wait(1)
-    for event in (0, 1, 2):
-        ups.wait_over(event)
+    ups.wait_over(0, 1, 3)
     expand(groups[0], True, False, 0, 3)
-    ups.last(0)
-    for event in (3, 4):
-        ups.wait_over(event)
+    ups.wait_over(2, 4)
     expand(groups[1], False, False, 0, 3)
-    ups.cross(2)
+    ups.wide(1)
+    ups.cross()
     downs.first()
+    ups.wait_over(5)
+    expand(groups[2], False, False, 0, 3)
     token_wait(2)
     expand(groups[0], True, False, 3, 4)
     expand(groups[1], False, False, 3, 4)
-    ups.last(-1)
-    for event in (5, 6):
-        ups.wait_over(event)
-    expand(groups[2], False, False, 0, 4)
-    ups.last(1)
-    ups.last(2)
-    for event in (7, 8, 9, 10):
-        ups.wait_over(event)
-    expand(groups[3], False, True, 0, 4)
+    expand(groups[2], False, False, 3, 4)
+    ups.edge()
+    ups.wait_over(6)
+    expand(groups[3], False, False, 0, 4)
+    ups.end()
+    ups.wait_over(7, 8)
+    expand(groups[4], False, True, 0, 4)
 
     def spot(dz, dy):
         return ring(z, dz) * SIDE + ring(y, dy)
 
-    def one_copy(pair, way):
+    def level_of(ref, unit, way, at_row):
+        return ref[unit, way, at_row:at_row + 16].astype(jnp.float32)[0:1]
+
+    def terms(shard, first, last):
+        return acc[shard // 2, first:last, (shard % 2) * width:(shard % 2 + 1) * width]
+
+    mid = rows // 2
+
+    def one_copy(unit, way):
+        span = pl.ds(0, len(units[unit]) * mid + 16)
         return remote(
-            one_out.at[pair, way], one_in.at[pair, way], one_send, one_recv.at[pair], at(0, 0, 1 - 2 * way)
+            one_out.at[unit, way, span], one_in.at[unit, way, span], one_send.at[unit], one_recv.at[unit],
+            at(0, 0, ways[way]),
         )
 
-    def two_copy(pair, way):
+    def two_copy(unit, way):
+        span = pl.ds(0, len(units[unit]) * rows + 16)
         return remote(
-            two_out.at[pair, way], two_in.at[pair, way], two_send, two_recv.at[pair], at(0, 0, 1 - 2 * way)
+            two_out.at[unit, way, span], two_in.at[unit, way, span], two_send.at[unit], two_recv.at[unit],
+            at(0, 0, ways[way]),
         )
 
-    def project(pair):
-        numbers = [spot(*place) for place in pairs[pair]]
+    def project(first, count):
+        numbers = [spot(*place) for place in shards_at[first:first + count]]
         left = jnp.concatenate([hidden[slot] for slot in range(2 * QUARTERS)], axis=1)
         right = jnp.concatenate([
             jnp.concatenate([down[core, f, q] for f in numbers], axis=1) for core in (0, 1) for q in range(QUARTERS)
         ], axis=0)
-        acc[pair] = jnp.dot(left, right, preferred_element_type=jnp.float32)
+        total = jnp.dot(left, right, preferred_element_type=jnp.float32)
+        for n in range(count):
+            shard = first + n
+            acc[shard // 2, :, (shard % 2) * width:(shard % 2 + 1) * width] = total[:, n * width:(n + 1) * width]
+
+    def launch(unit):
         for way in (0, 1):
-            (code,), level = encode(acc[pair, 3 * rows:, way * width:(way + 1) * width])
-            one_out[pair, way, 0:rows] = code
-            one_out[pair, way, rows:rows + 16] = level
-            one_copy(pair, way).start()
-
-    def relay(pair):
-        ref = one_in.at[pair]
-        remote(ref, ref, one_send, one_recv.at[pair], sibling).wait_recv()
+            first = 3 * rows + way * mid
+            codes, level = encode(jnp.concatenate([terms(shard, first, first + mid) for shard in units[unit]], axis=1))
+            for n, code in enumerate(codes):
+                one_out[unit, way, n * mid:(n + 1) * mid] = code
+            one_out[unit, way, len(codes) * mid:len(codes) * mid + 16] = level
+            one_copy(unit, way).start()
+
+    def relay(unit):
+        count = len(units[unit])
+        ref = one_in.at[unit, :, pl.ds(0, count * mid + 16)]
+        remote(ref, ref, one_send.at[unit], one_recv.at[unit], sibling).wait_recv()
         for way in (0, 1):
-            level = one_in[pair, way, rows:rows + 16].astype(jnp.float32)[0:1]
-            taken = decode(one_in[pair, way, 0:rows], level)
-            halves = [acc[pair, (1 + way) * rows:(2 + way) * rows, n * width:(n + 1) * width] for n in (0, 1)]
-            halves[way] = halves[way] + taken
-            codes, level = encode(jnp.concatenate(halves, axis=1))
-            for n in (0, 1):
-                two_out[pair, way, n * rows:(n + 1) * rows] = codes[n]
-            two_out[pair, way, 2 * rows:2 * rows + 16] = level
-            two_copy(pair, way).start()
-
-    def finish(pair):
-        ref = two_in.at[pair]
-        remote(ref, ref, two_send, two_recv.at[pair], sibling).wait_recv()
-        levels = [two_in[pair, way, 2 * rows:2 * rows + 16].astype(jnp.float32)[0:1] for way in (0, 1)]
-        for n, place in enumerate(pairs[pair]):
-            total = acc[pair, 0:rows, n * width:(n + 1) * width]
+            level = level_of(one_in, unit, way, count * mid)
+            sums = []
+            for n, shard in enumerate(units[unit]):
+                taken = decode(one_in[unit, way, n * mid:(n + 1) * mid], level)
+                halves = [terms(shard, (1 + way) * rows + part * mid, (1 + way) * rows + (part + 1) * mid) for part in (0, 1)]
+                halves[way] = halves[way] + taken
+                sums.append(jnp.concatenate(halves, axis=0))
+            codes, level = encode(jnp.concatenate(sums, axis=1))
+            for n, code in enumerate(codes):
+                two_out[unit, way, n * rows:(n + 1) * rows] = code
+            two_out[unit, way, count * rows:count * rows + 16] = level
+            two_copy(unit, way).start()
+
+    def finish(unit):
+        count = len(units[unit])
+        ref = two_in.at[unit, :, pl.ds(0, count * rows + 16)]
+        remote(ref, ref, two_send.at[unit], two_recv.at[unit], sibling).wait_recv()
+        levels = [level_of(two_in, unit, way, count * rows) for way in (0, 1)]
+        for n, shard in enumerate(units[unit]):
+            total = terms(shard, 0, rows)
             for way in (0, 1):
-                total = total + decode(two_in[pair, way, n * rows:(n + 1) * rows], levels[way])
-            out_ref[:, pl.ds(pl.multiple_of(spot(*place) * width, width), width)] = total.astype(jnp.bfloat16)
-
-    pairs = [
-        [(0, 0), (-1, 0)], [(1, 0), (0, -1)], [(0, 1), (2, 0)], [(0, 2), (-1, -1)],
-        [(-1, 1), (1, -1)], [(1, 1), (2, 1)], [(2, -1), (1, 2)], [(-1, 2), (2, 2)],
+                total = total + decode(two_in[unit, way, n * rows:(n + 1) * rows], levels[way])
+            f = spot(*shards_at[shard])
+            out_ref[:, pl.ds(pl.multiple_of(f * width, width), width)] = total.astype(jnp.bfloat16)
+
+    shards_at = [
+        (0, 0), (-1, 0), (1, 0), (0, -1), (0, 1), (2, 0), (0, 2), (-1, -1), (-1, 1), (1, -1), (1, 1),
+        (-1, 2), (2, -1), (1, 2), (2, 1), (2, 2),
     ]
+    units = [(0, 1), (2, 3), (4, 5, 6), (7, 8), (9, 10), (11, 12), (13, 14), (15,)]
+
     downs.near()
-    downs.cross(0)
-    for event in (0, 1, 3):
-        downs.wait_over(event)
-    project(0)
+    downs.own()
     downs.far()
-    project(1)
-    downs.cross(-1)
+    downs.wait_over(0, 1, 2)
+    project(0, 4)
+    launch(0)
+    launch(1)
+    downs.wide(0)
+    downs.back()
+    downs.wait_over(3, 4)
+    project(4, 3)
+    launch(2)
+    downs.wide(1)
     relay(0)
-    downs.cross(1)
-    downs.last(0)
     relay(1)
-    for event in (2, 4, 5, 7):
-        downs.wait_over(event)
-    project(2)
-    downs.cross(2)
-    project(3)
+    downs.cross()
+    downs.wait_over(5)
+    project(7, 4)
+    launch(3)
+    launch(4)
+    downs.edge()
     relay(2)
-    project(4)
-    relay(3)
+    downs.end()
     finish(0)
     finish(1)
+    downs.wait_over(6, 7)
+    project(11, 4)
+    launch(5)
+    launch(6)
+    relay(3)
     relay(4)
+    downs.wait_over(8)
+    project(15, 1)
+    launch(7)
     finish(2)
-    for ia in (-1, 1, 2):
-        downs.last(ia)
-    for event in (6, 8, 9, 10):
-        downs.wait_over(event)
-    project(5)
-    project(6)
-    relay(5)
-    project(7)
-    relay(6)
-    finish(3)
-    relay(7)
-    finish(4)
-    finish(5)
-    finish(6)
-    finish(7)
+    for unit in (5, 6, 7):
+        relay(unit)
+    for unit in (3, 4, 5, 6, 7):
+        finish(unit)
 
     ref = tok.at[pl.ds(0, 3)]
     remote(ref, ref, tok_send, tok_send, sibling).wait_send()
-    remote(one_out, one_out, one_send, one_send, sibling).wait_send()
-    remote(two_out, two_out, two_send, two_send, sibling).wait_send()
+    for unit in range(len(units)):
+        for way in (0, 1):
+            one_copy(unit, way).wait_send()
+            two_copy(unit, way).wait_send()
     ups.drain()
     downs.drain()
 
@@ -387,12 +437,12 @@
                 vm((2, fs, QUARTERS, piece, width), low),
                 vm((2 * QUARTERS, groups * rows, piece), full),
                 vm((2 * QUARTERS, groups * rows, piece), low),
-                vm((pairs, 2, rows + 16, LANES), low),
-                vm((pairs, 2, rows + 16, LANES), low),
-                vm((pairs, 2, 2 * rows + 16, LANES), low),
-                vm((pairs, 2, 2 * rows + 16, LANES), low),
+                vm((pairs, 2, 2 * rows, LANES), low),
+                vm((pairs, 2, 2 * rows, LANES), low),
+                vm((pairs, 2, 4 * rows, LANES), low),
+                vm((pairs, 2, 4 * rows, LANES), low),
                 dma((4,)), dma, dma((3,)),
-                dma((2, 15)), dma((2, 11)), dma((2,)), dma((2,)), dma, dma((pairs,)), dma, dma((pairs,)),
+                dma((2, 13)), dma((2, 9)), dma((2,)), dma((2,)), dma((pairs,)), dma((pairs,)), dma((pairs,)), dma((pairs,)),
             ],
             compiler_params=pltpu.CompilerParams(
                 collective_id=0, has_side_effects=True, vmem_limit_bytes=VMEM_LIMIT

time: 76 us -> 68.7 us (0.904); the launches traced: 75.8 us -> 67.6 us
  Pallas kernels: 74 us -> 65.7 us
    pallas_call x1, Pallas kernels: 74 us -> 65.7 us  [whole(): pl.pallas_call(kernel, out_shape=jax.ShapeDtypeStruct((rows, depth), low)...]
where the time goes in v3:
time: 68.7 us; the launch traced here: 67.6 us
  Pallas kernels  65.7 us (96%)
  local copies, waits for them, and re-layouts  1.88 us (3%)
    pallas_call x1, Pallas kernels, whole(): pl.pallas_call(kernel, out_shape=jax.ShapeDtypeStruct((rows, depth), low)...  65.7 us
    unnamed x1, local copies, waits for them, and re-layouts  1.88 us

profile of v3, /device:TPU:1, one launch (start us, length us, event | category | flops | bytes accessed | tf_op | source)
XLA Modules:
  0.0 67.6 jit_solution(6193514307816958118)
XLA Ops:
  0.0 65.7 %shard_map.46 = bf16[128,2048]{1,0:T(8,128)(2,1)} custom-call(bf16[128,2048]{1,0:T(8,128)(2,1)} %tok_hbm.1, f32[1,2048]{1,0:T(1,128)} %bitcast.1, f32[128,1024]{1,0:T(8,128)} %up_hbm.1, f32[1024,128]{1,0:T(8,128)} %down_hbm.1), custom_call_target="tpu_custom_call" | custom-call | tf_op jit(solution)/shard_map/pallas_call | solution.py:425
  65.7 1.9 %copy.6 = bf16[128,2048]{1,0:T(8,128)(2,1)} copy(bf16[128,2048]{1,0:T(8,128)(2,1)} %shard_map.46) | data formatting | bytes 1048576

commit v4 on v3

--- a/solution.py
+++ b/solution.py
@@ -9,10 +9,11 @@
 
 epsilon = 1e-06
 MESH = pl.DeviceIdType.MESH
-VMEM_LIMIT = 60_000_000
+VMEM_LIMIT = 56_020_000
 SIDE = 4
 QUARTERS = 4
 LANES = 128
+UNITS = 9
 POWER = 9
 PEAK = 11585.0
 TINY = 1e-30
@@ -69,7 +70,7 @@
         )
 
     barrier = pltpu.get_barrier_semaphore()
-    peers = [at(1, 0, 0), at(-1, 0, 0), at(0, 1, 0), at(0, -1, 0), at(0, 0, 1), at(0, 0, -1), sibling]
+    peers = [at(1, 0, 0), at(-1, 0, 0), at(0, 1, 0), at(0, -1, 0), at(0, 0, 1), at(0, 0, -1), at(0, 0, 2), sibling]
     for to in peers:
         pl.semaphore_signal(barrier, inc=1, device_id=to, device_id_type=MESH)
 
@@ -101,11 +102,9 @@
             ref = self.buf.at[c, pl.ds(0, count), 0]
             remote(ref, ref, sent.at[self.number], arrived.at[self.number, group], sibling).wait_recv()
 
-        def over(self, places, event):
-            for h in (0, 1):
-                for ia, ib in places:
-                    ref = self.buf.at[c, block(h, ia, ib), pl.ds(2 * h, 2)]
-                    remote(ref, ref, side_sent.at[self.number], crossed.at[self.number, event], sibling).start()
+        def over(self, h, ia, ib, j, event):
+            ref = self.buf.at[c, block(h, ia, ib), 2 * h + j]
+            remote(ref, ref, side_sent.at[self.number], crossed.at[self.number, event], sibling).start()
 
         def wait_over(self, *events):
             for event in events:
@@ -118,7 +117,9 @@
                     for h in (0, 1):
                         for s in ways:
                             self.send(h, 0, 0, turn if s > 0 else 1 - turn, axis, s, group + turn)
-            self.over([(0, 0)], 0)
+            for h in (0, 1):
+                for j in (0, 1):
+                    self.over(h, 0, 0, j, 0)
 
         def out(self, turn):
             for h in (0, 1):
@@ -126,23 +127,26 @@
                     for s in ways:
                         self.send(h, ia, 0, turn if ia < 0 else 1 - turn, "b", s, WIDE + turn)
 
-        def near(self):
-            self.wait(NEAR)
+        def near(self, turn):
+            self.wait(NEAR + turn)
+            if turn == 0:
+                for h in (0, 1):
+                    for s in ways:
+                        self.send(h, -s, 0, 0 if s > 0 else 1, "a", s, FAR)
+            self.out(turn)
             for h in (0, 1):
                 for s in ways:
-                    self.send(h, -s, 0, 0 if s > 0 else 1, "a", s, FAR)
-            self.out(0)
-            self.wait(NEAR + 1)
-            self.over([(-1, 0), (1, 0)], 1)
-
-        def own(self):
-            self.wait(OWN)
+                    self.over(h, -s, 0, turn if s > 0 else 1 - turn, 1)
+
+        def own(self, turn):
+            self.wait(OWN + turn)
+            if turn == 0:
+                for h in (0, 1):
+                    for s in ways:
+                        self.send(h, 0, -s, 0 if s > 0 else 1, "b", s, BACK)
             for h in (0, 1):
                 for s in ways:
-                    self.send(h, 0, -s, 0 if s > 0 else 1, "b", s, BACK)
-            self.out(1)
-            self.wait(OWN + 1)
-            self.over([(0, -1), (0, 1)], 2)
+                    self.over(h, 0, -s, turn if s > 0 else 1 - turn, 2)
 
         def far(self):
             self.wait(FAR)
@@ -150,36 +154,47 @@
                 for h in (0, 1):
                     for s in ways:
                         self.send(h, 2, 0, turn if s > 0 else 1 - turn, "b", s, CROSS + turn)
-            self.over([(2, 0)], 3)
+            for h in (0, 1):
+                for j in (0, 1):
+                    self.over(h, 2, 0, j, 3)
 
         def back(self):
             self.wait(BACK)
-            self.over([(0, 2)], 4)
+            for h in (0, 1):
+                for j in (0, 1):
+                    self.over(h, 0, 2, j, 4)
 
         def wide(self, turn):
             self.wait(WIDE + turn, 8)
             for h in (0, 1):
                 for s in ways:
                     self.send(h, -s if turn == 0 else s, -s, 0 if s > 0 else 1, "b", s, EDGE + turn)
-            if turn == 1:
-                self.over([(-1, -1), (-1, 1), (1, -1), (1, 1)], 5)
-
-        def cross(self):
-            self.wait(CROSS)
+            for h in (0, 1):
+                for ia in (-1, 1):
+                    for s in ways:
+                        self.over(h, ia, -s, turn if ia < 0 else 1 - turn, 5)
+
+        def cross(self, turn):
+            self.wait(CROSS + turn)
+            if turn == 0:
+                for h in (0, 1):
+                    for s in ways:
+                        self.send(h, 2, -s, 0 if s > 0 else 1, "b", s, END)
             for h in (0, 1):
                 for s in ways:
-                    self.send(h, 2, -s, 0 if s > 0 else 1, "b", s, END)
-            self.wait(CROSS + 1)
-            self.over([(2, -1), (2, 1)], 6)
-
-        def edge(self):
-            self.wait(EDGE)
-            self.wait(EDGE + 1)
-            self.over([(-1, 2), (1, 2)], 7)
+                    self.over(h, 2, -s, turn if s > 0 else 1 - turn, 6)
+
+        def edge(self, turn):
+            self.wait(EDGE + turn)
+            for h in (0, 1):
+                for s in ways:
+                    self.over(h, -s if turn == 0 else s, 2, 0 if s > 0 else 1, 7)
 
         def end(self):
             self.wait(END)
-            self.over([(2, 2)], 8)
+            for h in (0, 1):
+                for j in (0, 1):
+                    self.over(h, 2, 2, j, 8)
 
         def drain(self):
             ref = self.buf.at[0, pl.ds(0, self.buf.shape[1] - 1)]
@@ -245,38 +260,45 @@
                         acc[slot, span] = new
 
     groups = [
-        [(0, 0), (-1, 0), (1, 0), (2, 0)], [(0, -1), (0, 1), (0, 2)], [(-1, -1), (-1, 1), (1, -1), (1, 1)],
-        [(2, -1), (2, 1)], [(-1, 2), (1, 2), (2, 2)],
+        [(0, 0), (-1, 0), (1, 0), (2, 0)], [(-1, -1), (-1, 1), (1, -1), (1, 1)], [(0, -1), (0, 1)],
+        [(2, -1), (2, 1)], [(-1, 2), (1, 2)], [(0, 2), (2, 2)],
     ]
 
-    ups.near()
-    ups.own()
+    ups.near(0)
+    ups.near(1)
+    ups.own(0)
+    ups.own(1)
     ups.far()
     token_wait(0)
     for s in ways:
         token_send(ring(x, -s), 0 if s > 0 else 1, s, 2)
     ups.wide(0)
-    ups.back()
     token_wait(1)
     ups.wait_over(0, 1, 3)
     expand(groups[0], True, False, 0, 3)
-    ups.wait_over(2, 4)
+    ups.wide(1)
+    ups.back()
+    ups.wait_over(5)
     expand(groups[1], False, False, 0, 3)
-    ups.wide(1)
-    ups.cross()
+    ups.cross(0)
+    ups.wait_over(2)
+    expand(groups[2], False, False, 0, 3)
+    ups.cross(1)
     downs.first()
-    ups.wait_over(5)
-    expand(groups[2], False, False, 0, 3)
     token_wait(2)
     expand(groups[0], True, False, 3, 4)
     expand(groups[1], False, False, 3, 4)
     expand(groups[2], False, False, 3, 4)
-    ups.edge()
+    ups.edge(0)
+    ups.edge(1)
     ups.wait_over(6)
     expand(groups[3], False, False, 0, 4)
     ups.end()
-    ups.wait_over(7, 8)
-    expand(groups[4], False, True, 0, 4)
+    ups.wait_over(7)
+    expand(groups[4], False, False, 0, 4)
+    downs.near(0)
+    ups.wait_over(4, 8)
+    expand(groups[5], False, True, 0, 4)
 
     def spot(dz, dy):
         return ring(z, dz) * SIDE + ring(y, dy)
@@ -296,6 +318,12 @@
             at(0, 0, ways[way]),
         )
 
+    def far_copy(unit):
+        span = pl.ds(0, len(units[unit]) * rows + 16)
+        return remote(
+            one_out.at[unit, 0, span], one_in.at[unit, 0, span], one_send.at[unit], one_recv.at[unit], at(0, 0, 2)
+        )
+
     def two_copy(unit, way):
         span = pl.ds(0, len(units[unit]) * rows + 16)
         return remote(
@@ -305,23 +333,40 @@
 
     def project(first, count):
         numbers = [spot(*place) for place in shards_at[first:first + count]]
-        left = jnp.concatenate([hidden[slot] for slot in range(2 * QUARTERS)], axis=1)
         right = jnp.concatenate([
             jnp.concatenate([down[core, f, q] for f in numbers], axis=1) for core in (0, 1) for q in range(QUARTERS)
         ], axis=0)
-        total = jnp.dot(left, right, preferred_element_type=jnp.float32)
-        for n in range(count):
-            shard = first + n
-            acc[shard // 2, :, (shard % 2) * width:(shard % 2 + 1) * width] = total[:, n * width:(n + 1) * width]
+        parts = 1 if count > 2 else 2
+        tall = 4 * rows // parts
+        for part in range(parts):
+            span = slice(part * tall, (part + 1) * tall)
+            left = jnp.concatenate([hidden[slot, span] for slot in range(2 * QUARTERS)], axis=1)
+            total = jnp.dot(left, right, preferred_element_type=jnp.float32)
+            for n in range(count):
+                shard = first + n
+                acc[shard // 2, span, (shard % 2) * width:(shard % 2 + 1) * width] = total[:, n * width:(n + 1) * width]
+
+    def pack(ref, unit, way, codes, level):
+        tall = codes[0].shape[0]
+        for n, code in enumerate(codes):
+            ref[unit, way, n * tall:(n + 1) * tall] = code
+        ref[unit, way, len(codes) * tall:len(codes) * tall + 16] = level
+
+    def gather_terms(unit, first, last):
+        return jnp.concatenate([terms(shard, first, last) for shard in units[unit]], axis=1)
 
     def launch(unit):
-        for way in (0, 1):
-            first = 3 * rows + way * mid
-            codes, level = encode(jnp.concatenate([terms(shard, first, first + mid) for shard in units[unit]], axis=1))
-            for n, code in enumerate(codes):
-                one_out[unit, way, n * mid:(n + 1) * mid] = code
-            one_out[unit, way, len(codes) * mid:len(codes) * mid + 16] = level
-            one_copy(unit, way).start()
+        if unit in direct:
+            pack(one_out, unit, 0, *encode(gather_terms(unit, 3 * rows, 4 * rows)))
+            far_copy(unit).start()
+            for way in (0, 1):
+                pack(two_out, unit, way, *encode(gather_terms(unit, (1 + way) * rows, (2 + way) * rows)))
+                two_copy(unit, way).start()
+        else:
+            for way in (0, 1):
+                first = 3 * rows + way * mid
+                pack(one_out, unit, way, *encode(gather_terms(unit, first, first + mid)))
+                one_copy(unit, way).start()
 
     def relay(unit):
         count = len(units[unit])
@@ -335,76 +380,87 @@
                 halves = [terms(shard, (1 + way) * rows + part * mid, (1 + way) * rows + (part + 1) * mid) for part in (0, 1)]
                 halves[way] = halves[way] + taken
                 sums.append(jnp.concatenate(halves, axis=0))
-            codes, level = encode(jnp.concatenate(sums, axis=1))
-            for n, code in enumerate(codes):
-                two_out[unit, way, n * rows:(n + 1) * rows] = code
-            two_out[unit, way, count * rows:count * rows + 16] = level
+            pack(two_out, unit, way, *encode(jnp.concatenate(sums, axis=1)))
             two_copy(unit, way).start()
 
     def finish(unit):
         count = len(units[unit])
         ref = two_in.at[unit, :, pl.ds(0, count * rows + 16)]
         remote(ref, ref, two_send.at[unit], two_recv.at[unit], sibling).wait_recv()
-        levels = [level_of(two_in, unit, way, count * rows) for way in (0, 1)]
+        incoming = [(two_in, 0), (two_in, 1)]
+        if unit in direct:
+            far_copy(unit).wait_recv()
+            incoming.append((one_in, 0))
+        levels = [level_of(buf, unit, way, count * rows) for buf, way in incoming]
         for n, shard in enumerate(units[unit]):
             total = terms(shard, 0, rows)
-            for way in (0, 1):
-                total = total + decode(two_in[unit, way, n * rows:(n + 1) * rows], levels[way])
+            for (buf, way), level in zip(incoming, levels):
+                total = total + decode(buf[unit, way, n * rows:(n + 1) * rows], level)
             f = spot(*shards_at[shard])
             out_ref[:, pl.ds(pl.multiple_of(f * width, width), width)] = total.astype(jnp.bfloat16)
 
     shards_at = [
-        (0, 0), (-1, 0), (1, 0), (0, -1), (0, 1), (2, 0), (0, 2), (-1, -1), (-1, 1), (1, -1), (1, 1),
+        (0, 0), (-1, 0), (1, 0), (0, -1), (0, 1), (-1, -1), (-1, 1), (1, -1), (1, 1), (2, 0), (0, 2),
         (-1, 2), (2, -1), (1, 2), (2, 1), (2, 2),
     ]
-    units = [(0, 1), (2, 3), (4, 5, 6), (7, 8), (9, 10), (11, 12), (13, 14), (15,)]
-
-    downs.near()
-    downs.own()
+    units = [(0,), (1, 2), (3, 4), (5, 6), (7, 8), (9, 10), (11, 12), (13, 14), (15,)]
+    direct = (0, 1, 2)
+
+    downs.near(1)
+    downs.wait_over(0)
+    project(0, 1)
+    launch(0)
+    downs.own(0)
+    downs.own(1)
     downs.far()
-    downs.wait_over(0, 1, 2)
-    project(0, 4)
-    launch(0)
+    downs.wait_over(1, 2)
+    project(1, 4)
     launch(1)
+    launch(2)
     downs.wide(0)
+    downs.wide(1)
+    finish(0)
+    downs.wait_over(5)
+    project(5, 4)
+    launch(3)
+    launch(4)
     downs.back()
     downs.wait_over(3, 4)
-    project(4, 3)
-    launch(2)
-    downs.wide(1)
-    relay(0)
-    relay(1)
-    downs.cross()
-    downs.wait_over(5)
-    project(7, 4)
-    launch(3)
-    launch(4)
-    downs.edge()
-    relay(2)
-    downs.end()
-    finish(0)
+    project(9, 2)
+    launch(5)
+    downs.cross(0)
+    downs.cross(1)
+    downs.edge(0)
+    relay(3)
+    relay(4)
+    downs.edge(1)
     finish(1)
+    finish(2)
     downs.wait_over(6, 7)
     project(11, 4)
-    launch(5)
     launch(6)
-    relay(3)
-    relay(4)
+    launch(7)
+    if 5 not in direct:
+        relay(5)
+    downs.end()
     downs.wait_over(8)
     project(15, 1)
-    launch(7)
-    finish(2)
-    for unit in (5, 6, 7):
-        relay(unit)
-    for unit in (3, 4, 5, 6, 7):
+    launch(8)
+    for unit in (6, 7, 8):
+        if unit not in direct:
+            relay(unit)
+    for unit in (3, 4, 5, 6, 7, 8):
         finish(unit)
 
     ref = tok.at[pl.ds(0, 3)]
     remote(ref, ref, tok_send, tok_send, sibling).wait_send()
     for unit in range(len(units)):
         for way in (0, 1):
-            one_copy(unit, way).wait_send()
             two_copy(unit, way).wait_send()
+            if unit not in direct:
+                one_copy(unit, way).wait_send()
+        if unit in direct:
+            far_copy(unit).wait_send()
     ups.drain()
     downs.drain()
 
@@ -421,7 +477,6 @@
         groups = tp // 2
         vm, dma = pltpu.VMEM, pltpu.SemaphoreType.DMA
         low, full = jnp.bfloat16, jnp.float32
-        pairs = fs // 2
         return pl.pallas_call(
             kernel,
             out_shape=jax.ShapeDtypeStruct((rows, depth), low),
@@ -437,12 +492,12 @@
                 vm((2, fs, QUARTERS, piece, width), low),
                 vm((2 * QUARTERS, groups * rows, piece), full),
                 vm((2 * QUARTERS, groups * rows, piece), low),
-                vm((pairs, 2, 2 * rows, LANES), low),
-                vm((pairs, 2, 2 * rows, LANES), low),
-                vm((pairs, 2, 4 * rows, LANES), low),
-                vm((pairs, 2, 4 * rows, LANES), low),
+                vm((UNITS, 2, 2 * rows + 16, LANES), low),
+                vm((UNITS, 2, 2 * rows + 16, LANES), low),
+                vm((UNITS, 2, 2 * rows + 16, LANES), low),
+                vm((UNITS, 2, 2 * rows + 16, LANES), low),
                 dma((4,)), dma, dma((3,)),
-                dma((2, 13)), dma((2, 9)), dma((2,)), dma((2,)), dma((pairs,)), dma((pairs,)), dma((pairs,)), dma((pairs,)),
+                dma((2, 13)), dma((2, 9)), dma((2,)), dma((2,)), dma((UNITS,)), dma((UNITS,)), dma((UNITS,)), dma((UNITS,)),
             ],
             compiler_params=pltpu.CompilerParams(
                 collective_id=0, has_side_effects=True, vmem_limit_bytes=VMEM_LIMIT

time: 68.7 us -> 64.9 us (0.945); the launches traced: 67.6 us -> 64.8 us
  Pallas kernels: 65.7 us -> 63.3 us
    pallas_call x1, Pallas kernels: 65.7 us -> 63.3 us  [whole(): pl.pallas_call(kernel, out_shape=jax.ShapeDtypeStruct((rows, depth), low)...]
    unnamed x1 -> x3, local copies, waits for them, and re-layouts: 1.88 us -> 1.49 us
where the time goes in v4:
time: 64.9 us; the launch traced here: 64.8 us
  Pallas kernels  63.3 us (98%)
  local copies, waits for them, and re-layouts  1.49 us (2%)
    pallas_call x1, Pallas kernels, whole(): pl.pallas_call(kernel, out_shape=jax.ShapeDtypeStruct((rows, depth), low)...  63.3 us
    unnamed x3, local copies, waits for them, and re-layouts  1.49 us

profile of v4, /device:TPU:1, one launch (start us, length us, event | category | flops | bytes accessed | tf_op | source)
XLA Modules:
  0.0 64.8 jit_solution(15650288750605045516)
XLA Ops:
  0.0 0.0 copy-start
  0.0 0.7 %copy-done = f32[2048]{0:T(1024)S(1)} copy-done((f32[2048]{0:T(1024)S(1)}, f32[2048]{0:T(1024)}, u32[]{:S(2)}) %copy-start) | copy-done | bytes 8216
  0.7 63.3 %shard_map.46 = bf16[128,2048]{1,0:T(8,128)(2,1)S(1)} custom-call(bf16[128,2048]{1,0:T(8,128)(2,1)} %tok_hbm.1, f32[1,2048]{1,0:T(1,128)S(1)} %bitcast.1, f32[128,1024]{1,0:T(8,128)} %up_hbm.1, f32[1024,128]{1,0:T(8,128)} %down_hbm.1), custom_call_target="tpu_custom_call" | custom-call | tf_op jit(solution)/shard_map/pallas_call | solution.py:480
  64.0 0.8 %copy.6 = bf16[128,2048]{1,0:T(8,128)(2,1)} copy(bf16[128,2048]{1,0:T(8,128)(2,1)S(1)} %shard_map.46) | data formatting | bytes 1048576
Async XLA Ops:
  0.0 0.7 %copy-start = (f32[2048]{0:T(1024)S(1)}, f32[2048]{0:T(1024)}, u32[]{:S(2)}) copy-start(f32[2048]{0:T(1024)} %param.5) | copy-start | bytes 24580

commit v5 on v4

--- a/solution.py
+++ b/solution.py
@@ -9,7 +9,7 @@
 
 epsilon = 1e-06
 MESH = pl.DeviceIdType.MESH
-VMEM_LIMIT = 56_020_000
+VMEM_LIMIT = 48_000_000
 SIDE = 4
 QUARTERS = 4
 LANES = 128
@@ -32,7 +32,7 @@
         t2 = t * t
         t4 = t2 * t2
         codes.append((t4 * t4 * t).astype(jnp.bfloat16))
-    return codes, jnp.broadcast_to(level, (16, LANES))
+    return codes, jnp.broadcast_to(level, (8, LANES))
 
 
 def decode(code, level):
@@ -86,11 +86,11 @@
         return ring(z, dz) * SIDE + ring(y, dy)
 
     ways = (1, -1)
-    NEAR, OWN, FAR, BACK, WIDE, EDGE, CROSS, END = 0, 2, 4, 5, 6, 8, 10, 12
+    NEAR, OWN, FAR, BACK, WIDE, MID, LATE, END = 0, 2, 4, 5, 6, 8, 10, 12
 
     class Gather:
-        def __init__(self, number, buf):
-            self.number, self.buf = number, buf
+        def __init__(self, number, buf, skew):
+            self.number, self.buf, self.skew = number, buf, skew
 
         def send(self, h, ia, ib, j, axis, s, group):
             along_z = (axis == "a") == (h == 0)
@@ -148,12 +148,17 @@
                 for s in ways:
                     self.over(h, 0, -s, turn if s > 0 else 1 - turn, 2)
 
+        def out_far(self, h, turn):
+            group = LATE + 1 if h == 1 and turn == 1 and self.skew else MID + turn
+            for s in ways:
+                self.send(h, 2, 0, turn if s > 0 else 1 - turn, "b", s, group)
+
         def far(self):
             self.wait(FAR)
             for turn in (0, 1):
                 for h in (0, 1):
-                    for s in ways:
-                        self.send(h, 2, 0, turn if s > 0 else 1 - turn, "b", s, CROSS + turn)
+                    if h == 0 or turn == 0 or not self.skew:
+                        self.out_far(h, turn)
             for h in (0, 1):
                 for j in (0, 1):
                     self.over(h, 2, 0, j, 3)
@@ -168,27 +173,46 @@
             self.wait(WIDE + turn, 8)
             for h in (0, 1):
                 for s in ways:
-                    self.send(h, -s if turn == 0 else s, -s, 0 if s > 0 else 1, "b", s, EDGE + turn)
+                    ia = -s if turn == 0 else s
+                    group = (MID + 1, LATE)[turn] if h == 1 and self.skew else LATE + turn
+                    self.send(h, ia, -s, 0 if s > 0 else 1, "b", s, group)
+            if turn == 1 and self.skew:
+                self.out_far(1, 1)
             for h in (0, 1):
                 for ia in (-1, 1):
                     for s in ways:
                         self.over(h, ia, -s, turn if ia < 0 else 1 - turn, 5)
 
-        def cross(self, turn):
-            self.wait(CROSS + turn)
+        def crossed_far(self, h, turn, event):
             if turn == 0:
-                for h in (0, 1):
-                    for s in ways:
-                        self.send(h, 2, -s, 0 if s > 0 else 1, "b", s, END)
-            for h in (0, 1):
                 for s in ways:
-                    self.over(h, 2, -s, turn if s > 0 else 1 - turn, 6)
-
-        def edge(self, turn):
-            self.wait(EDGE + turn)
-            for h in (0, 1):
-                for s in ways:
-                    self.over(h, -s if turn == 0 else s, 2, 0 if s > 0 else 1, 7)
+                    self.send(h, 2, -s, 0 if s > 0 else 1, "b", s, END)
+            for s in ways:
+                self.over(h, 2, -s, turn if s > 0 else 1 - turn, event)
+
+        def crossed_edge(self, h, turn, event):
+            for s in ways:
+                self.over(h, -s if turn == 0 else s, 2, 0 if s > 0 else 1, event)
+
+        def mid(self, turn):
+            self.wait(MID + turn)
+            self.crossed_far(0, turn, 6)
+            if not self.skew:
+                self.crossed_far(1, turn, 6)
+            elif turn == 0:
+                self.crossed_far(1, 0, 7)
+            else:
+                self.crossed_edge(1, 0, 6)
+
+        def late(self, turn):
+            self.wait(LATE + turn)
+            self.crossed_edge(0, turn, 7)
+            if not self.skew:
+                self.crossed_edge(1, turn, 7)
+            elif turn == 0:
+                self.crossed_edge(1, 1, 6)
+            else:
+                self.crossed_far(1, 1, 7)
 
         def end(self):
             self.wait(END)
@@ -202,8 +226,8 @@
             whole = self.buf.at[0]
             remote(whole, whole, side_sent.at[self.number], side_sent.at[self.number], sibling).wait_send()
 
-    ups = Gather(0, up)
-    downs = Gather(1, down)
+    ups = Gather(0, up, False)
+    downs = Gather(1, down, True)
 
     loads[0].wait()
     for q in range(QUARTERS):
@@ -280,17 +304,17 @@
     ups.back()
     ups.wait_over(5)
     expand(groups[1], False, False, 0, 3)
-    ups.cross(0)
+    ups.mid(0)
     ups.wait_over(2)
     expand(groups[2], False, False, 0, 3)
-    ups.cross(1)
+    ups.mid(1)
     downs.first()
     token_wait(2)
     expand(groups[0], True, False, 3, 4)
     expand(groups[1], False, False, 3, 4)
     expand(groups[2], False, False, 3, 4)
-    ups.edge(0)
-    ups.edge(1)
+    ups.late(0)
+    ups.late(1)
     ups.wait_over(6)
     expand(groups[3], False, False, 0, 4)
     ups.end()
@@ -304,7 +328,7 @@
         return ring(z, dz) * SIDE + ring(y, dy)
 
     def level_of(ref, unit, way, at_row):
-        return ref[unit, way, at_row:at_row + 16].astype(jnp.float32)[0:1]
+        return ref[unit, way, at_row:at_row + 8].astype(jnp.float32)[0:1]
 
     def terms(shard, first, last):
         return acc[shard // 2, first:last, (shard % 2) * width:(shard % 2 + 1) * width]
@@ -312,20 +336,20 @@
     mid = rows // 2
 
     def one_copy(unit, way):
-        span = pl.ds(0, len(units[unit]) * mid + 16)
+        span = pl.ds(0, len(units[unit]) * mid + 8)
         return remote(
             one_out.at[unit, way, span], one_in.at[unit, way, span], one_send.at[unit], one_recv.at[unit],
             at(0, 0, ways[way]),
         )
 
     def far_copy(unit):
-        span = pl.ds(0, len(units[unit]) * rows + 16)
+        span = pl.ds(0, len(units[unit]) * rows + 8)
         return remote(
             one_out.at[unit, 0, span], one_in.at[unit, 0, span], one_send.at[unit], one_recv.at[unit], at(0, 0, 2)
         )
 
     def two_copy(unit, way):
-        span = pl.ds(0, len(units[unit]) * rows + 16)
+        span = pl.ds(0, len(units[unit]) * rows + 8)
         return remote(
             two_out.at[unit, way, span], two_in.at[unit, way, span], two_send.at[unit], two_recv.at[unit],
             at(0, 0, ways[way]),
@@ -350,7 +374,7 @@
         tall = codes[0].shape[0]
         for n, code in enumerate(codes):
             ref[unit, way, n * tall:(n + 1) * tall] = code
-        ref[unit, way, len(codes) * tall:len(codes) * tall + 16] = level
+        ref[unit, way, len(codes) * tall:len(codes) * tall + 8] = level
 
     def gather_terms(unit, first, last):
         return jnp.concatenate([terms(shard, first, last) for shard in units[unit]], axis=1)
@@ -370,7 +394,7 @@
 
     def relay(unit):
         count = len(units[unit])
-        ref = one_in.at[unit, :, pl.ds(0, count * mid + 16)]
+        ref = one_in.at[unit, :, pl.ds(0, count * mid + 8)]
         remote(ref, ref, one_send.at[unit], one_recv.at[unit], sibling).wait_recv()
         for way in (0, 1):
             level = level_of(one_in, unit, way, count * mid)
@@ -385,7 +409,7 @@
 
     def finish(unit):
         count = len(units[unit])
-        ref = two_in.at[unit, :, pl.ds(0, count * rows + 16)]
+        ref = two_in.at[unit, :, pl.ds(0, count * rows + 8)]
         remote(ref, ref, two_send.at[unit], two_recv.at[unit], sibling).wait_recv()
         incoming = [(two_in, 0), (two_in, 1)]
         if unit in direct:
@@ -401,10 +425,10 @@
 
     shards_at = [
         (0, 0), (-1, 0), (1, 0), (0, -1), (0, 1), (-1, -1), (-1, 1), (1, -1), (1, 1), (2, 0), (0, 2),
-        (-1, 2), (2, -1), (1, 2), (2, 1), (2, 2),
+        (2, -1), (2, 1), (-1, 2), (1, 2), (2, 2),
     ]
     units = [(0,), (1, 2), (3, 4), (5, 6), (7, 8), (9, 10), (11, 12), (13, 14), (15,)]
-    direct = (0, 1, 2)
+    direct = (0, 1, 2, 5)
 
     downs.near(1)
     downs.wait_over(0)
@@ -425,24 +449,26 @@
     launch(3)
     launch(4)
     downs.back()
+    downs.mid(0)
     downs.wait_over(3, 4)
     project(9, 2)
     launch(5)
-    downs.cross(0)
-    downs.cross(1)
-    downs.edge(0)
+    downs.mid(1)
+    downs.late(0)
     relay(3)
     relay(4)
-    downs.edge(1)
+    downs.wait_over(6)
+    project(11, 2)
+    launch(6)
+    downs.late(1)
     finish(1)
     finish(2)
-    downs.wait_over(6, 7)
-    project(11, 4)
-    launch(6)
-    launch(7)
+    downs.end()
     if 5 not in direct:
         relay(5)
-    downs.end()
+    downs.wait_over(7)
+    project(13, 2)
+    launch(7)
     downs.wait_over(8)
     project(15, 1)
     launch(8)
@@ -492,17 +518,20 @@
                 vm((2, fs, QUARTERS, piece, width), low),
                 vm((2 * QUARTERS, groups * rows, piece), full),
                 vm((2 * QUARTERS, groups * rows, piece), low),
-                vm((UNITS, 2, 2 * rows + 16, LANES), low),
-                vm((UNITS, 2, 2 * rows + 16, LANES), low),
-                vm((UNITS, 2, 2 * rows + 16, LANES), low),
-                vm((UNITS, 2, 2 * rows + 16, LANES), low),
+                vm((UNITS, 2, 2 * rows + 8, LANES), low),
+                vm((UNITS, 2, 2 * rows + 8, LANES), low),
+                vm((UNITS, 2, 2 * rows + 8, LANES), low),
+                vm((UNITS, 2, 2 * rows + 8, LANES), low),
                 dma((4,)), dma, dma((3,)),
                 dma((2, 13)), dma((2, 9)), dma((2,)), dma((2,)), dma((UNITS,)), dma((UNITS,)), dma((UNITS,)), dma((UNITS,)),
             ],
             compiler_params=pltpu.CompilerParams(
                 collective_id=0, has_side_effects=True, vmem_limit_bytes=VMEM_LIMIT
             ),
-        )(tokens, norm_gain.reshape(1, depth), up_weight, down_weight)
+        )(*(
+            pltpu.with_memory_space_constraint(array, pltpu.HBM)
+            for array in (tokens, norm_gain.reshape(1, depth), up_weight, down_weight)
+        ))
 
     return jax.shard_map(
         whole, mesh=mesh, in_specs=placed, out_specs=P(("fs", "tp"), None), check_vma=False

time: 64.9 us -> 63.8 us (0.983)
  Pallas kernels: 63.3 us -> 62.2 us
  local copies, waits for them, and re-layouts: 1.49 us -> 0.8 us
    pallas_call x1, Pallas kernels: 63.3 us -> 62.2 us  [whole(): pl.pallas_call(kernel, out_shape=jax.ShapeDtypeStruct((rows, depth), low)...]
    unnamed x3 -> x1, local copies, waits for them, and re-layouts: 1.49 us -> 0.8 us
where the time goes in v5:
time: 63.8 us; the launch traced here: 63 us
  Pallas kernels  62.2 us (97%)
  local copies, waits for them, and re-layouts  0.8 us (1%)
    pallas_call x1, Pallas kernels, whole(): pl.pallas_call(kernel, out_shape=jax.ShapeDtypeStruct((rows, depth), low)...  62.2 us

profile of v5, /device:TPU:1, one launch (start us, length us, event | category | flops | bytes accessed | tf_op | source)
XLA Modules:
  0.0 63.0 jit_solution(16489833991139432649)
XLA Ops:
  0.0 62.2 %shard_map.46 = bf16[128,2048]{1,0:T(8,128)(2,1)S(1)} custom-call(bf16[128,2048]{1,0:T(8,128)(2,1)} %tok_hbm.1, f32[1,2048]{1,0:T(1,128)} %bitcast.1, f32[128,1024]{1,0:T(8,128)} %up_hbm.1, f32[1024,128]{1,0:T(8,128)} %down_hbm.1), custom_call_target="tpu_custom_call" | custom-call | tf_op jit(solution)/shard_map/pallas_call | solution.py:506
  62.2 0.8 %copy.6 = bf16[128,2048]{1,0:T(8,128)(2,1)} copy(bf16[128,2048]{1,0:T(8,128)(2,1)S(1)} %shard_map.46) | data formatting | bytes 1048576

commit v6 on v5

--- a/solution.py
+++ b/solution.py
@@ -428,7 +428,7 @@
         (2, -1), (2, 1), (-1, 2), (1, 2), (2, 2),
     ]
     units = [(0,), (1, 2), (3, 4), (5, 6), (7, 8), (9, 10), (11, 12), (13, 14), (15,)]
-    direct = (0, 1, 2, 5)
+    direct = (0, 1, 2)
 
     downs.near(1)
     downs.wait_over(0)
@@ -437,11 +437,13 @@
     downs.own(0)
     downs.own(1)
     downs.far()
-    downs.wait_over(1, 2)
+    downs.wait_over(1)
+    downs.wait_over(2)
     project(1, 4)
     launch(1)
     launch(2)
     downs.wide(0)
+    downs.wait_over(3)
     downs.wide(1)
     finish(0)
     downs.wait_over(5)
@@ -450,33 +452,36 @@
     launch(4)
     downs.back()
     downs.mid(0)
-    downs.wait_over(3, 4)
+    downs.wait_over(4)
     project(9, 2)
     launch(5)
     downs.mid(1)
     downs.late(0)
     relay(3)
-    relay(4)
     downs.wait_over(6)
     project(11, 2)
     launch(6)
+    relay(4)
     downs.late(1)
     finish(1)
     finish(2)
     downs.end()
-    if 5 not in direct:
-        relay(5)
     downs.wait_over(7)
     project(13, 2)
     launch(7)
     downs.wait_over(8)
     project(15, 1)
     launch(8)
-    for unit in (6, 7, 8):
-        if unit not in direct:
-            relay(unit)
-    for unit in (3, 4, 5, 6, 7, 8):
-        finish(unit)
+    relay(5)
+    relay(6)
+    relay(7)
+    relay(8)
+    finish(3)
+    finish(4)
+    finish(5)
+    finish(6)
+    finish(7)
+    finish(8)
 
     ref = tok.at[pl.ds(0, 3)]
     remote(ref, ref, tok_send, tok_send, sibling).wait_send()

time: 63.8 us -> 63.5 us (level); the launches traced: 63 us -> 63.4 us
  no operation moved by 1% of the time
where the time goes in v6:
time: 63.5 us; the launch traced here: 63.4 us
  Pallas kernels  62.6 us (99%)
  local copies, waits for them, and re-layouts  0.8 us (1%)
    pallas_call x1, Pallas kernels, whole(): pl.pallas_call(kernel, out_shape=jax.ShapeDtypeStruct((rows, depth), low)...  62.6 us

profile of v6, /device:TPU:1, one launch (start us, length us, event | category | flops | bytes accessed | tf_op | source)
XLA Modules:
  0.0 63.4 jit_solution(14055656714113846714)
XLA Ops:
  0.0 62.6 %shard_map.46 = bf16[128,2048]{1,0:T(8,128)(2,1)S(1)} custom-call(bf16[128,2048]{1,0:T(8,128)(2,1)} %tok_hbm.1, f32[1,2048]{1,0:T(1,128)} %bitcast.1, f32[128,1024]{1,0:T(8,128)} %up_hbm.1, f32[1024,128]{1,0:T(8,128)} %down_hbm.1), custom_call_target="tpu_custom_call" | custom-call | tf_op jit(solution)/shard_map/pallas_call | solution.py:511
  62.6 0.8 %copy.6 = bf16[128,2048]{1,0:T(8,128)(2,1)} copy(bf16[128,2048]{1,0:T(8,128)(2,1)S(1)} %shard_map.46) | data formatting | bytes 1048576

commit v7 on v6

--- a/solution.py
+++ b/solution.py
@@ -78,8 +78,7 @@
         pltpu.make_async_copy(src, dst, load.at[n])
         for n, (src, dst) in enumerate([(up_hbm, up_ref), (tok_hbm, tok_ref), (gain_hbm, gain_ref), (down_hbm, down_ref)])
     ]
-    for copy in loads:
-        copy.start()
+    loads[0].start()
 
     def block(h, ia, ib):
         dz, dy = (ia, ib) if h == 0 else (ib, ia)
@@ -230,6 +229,8 @@
     downs = Gather(1, down, True)
 
     loads[0].wait()
+    for copy in loads[1:]:
+        copy.start()
     for q in range(QUARTERS):
         up[c, mine, q] = up_ref[:, q * piece:(q + 1) * piece].astype(jnp.bfloat16)
     pl.semaphore_wait(barrier, len(peers))
@@ -428,7 +429,7 @@
         (2, -1), (2, 1), (-1, 2), (1, 2), (2, 2),
     ]
     units = [(0,), (1, 2), (3, 4), (5, 6), (7, 8), (9, 10), (11, 12), (13, 14), (15,)]
-    direct = (0, 1, 2)
+    direct = (0, 1, 2, 5)
 
     downs.near(1)
     downs.wait_over(0)
@@ -472,7 +473,6 @@
     downs.wait_over(8)
     project(15, 1)
     launch(8)
-    relay(5)
     relay(6)
     relay(7)
     relay(8)

time: 63.5 us -> 63.4 us (level)
  Pallas kernels: 62.6 us -> 61.9 us
    pallas_call x1, Pallas kernels: 62.6 us -> 61.9 us  [whole(): pl.pallas_call(kernel, out_shape=jax.ShapeDtypeStruct((rows, depth), low)...]
where the time goes in v7:
time: 63.4 us; the launch traced here: 62.7 us
  Pallas kernels  61.9 us (98%)
  local copies, waits for them, and re-layouts  0.8 us (1%)
    pallas_call x1, Pallas kernels, whole(): pl.pallas_call(kernel, out_shape=jax.ShapeDtypeStruct((rows, depth), low)...  61.9 us

profile of v7, /device:TPU:1, one launch (start us, length us, event | category | flops | bytes accessed | tf_op | source)
XLA Modules:
  0.0 62.7 jit_solution(7463764802988793315)
XLA Ops:
  0.0 61.9 %shard_map.46 = bf16[128,2048]{1,0:T(8,128)(2,1)S(1)} custom-call(bf16[128,2048]{1,0:T(8,128)(2,1)} %tok_hbm.1, f32[1,2048]{1,0:T(1,128)} %bitcast.1, f32[128,1024]{1,0:T(8,128)} %up_hbm.1, f32[1024,128]{1,0:T(8,128)} %down_hbm.1), custom_call_target="tpu_custom_call" | custom-call | tf_op jit(solution)/shard_map/pallas_call | solution.py:511
  61.9 0.8 %copy.6 = bf16[128,2048]{1,0:T(8,128)(2,1)} copy(bf16[128,2048]{1,0:T(8,128)(2,1)S(1)} %shard_map.46) | data formatting | bytes 1048576

commit v8 on v7

--- a/solution.py
+++ b/solution.py
@@ -70,7 +70,7 @@
         )
 
     barrier = pltpu.get_barrier_semaphore()
-    peers = [at(1, 0, 0), at(-1, 0, 0), at(0, 1, 0), at(0, -1, 0), at(0, 0, 1), at(0, 0, -1), at(0, 0, 2), sibling]
+    peers = [at(1, 0, 0), at(-1, 0, 0), at(0, 1, 0), at(0, -1, 0), at(0, 0, 1), at(0, 0, -1), sibling]
     for to in peers:
         pl.semaphore_signal(barrier, inc=1, device_id=to, device_id_type=MESH)
 

time: 63.4 us -> 63.6 us (level)
  no operation moved by 1% of the time
where the time goes in v8:
time: 63.6 us; the launch traced here: 62.9 us
  Pallas kernels  62.1 us (98%)
  local copies, waits for them, and re-layouts  0.8 us (1%)
    pallas_call x1, Pallas kernels, whole(): pl.pallas_call(kernel, out_shape=jax.ShapeDtypeStruct((rows, depth), low)...  62.1 us

profile of v8, /device:TPU:1, one launch (start us, length us, event | category | flops | bytes accessed | tf_op | source)
XLA Modules:
  0.0 62.9 jit_solution(14212111399267448447)
XLA Ops:
  0.0 62.1 %shard_map.46 = bf16[128,2048]{1,0:T(8,128)(2,1)S(1)} custom-call(bf16[128,2048]{1,0:T(8,128)(2,1)} %tok_hbm.1, f32[1,2048]{1,0:T(1,128)} %bitcast.1, f32[128,1024]{1,0:T(8,128)} %up_hbm.1, f32[1024,128]{1,0:T(8,128)} %down_hbm.1), custom_call_target="tpu_custom_call" | custom-call | tf_op jit(solution)/shard_map/pallas_call | solution.py:511
  62.1 0.8 %copy.6 = bf16[128,2048]{1,0:T(8,128)(2,1)} copy(bf16[128,2048]{1,0:T(8,128)(2,1)S(1)} %shard_map.46) | data formatting | bytes 1048576

commit v9 on v6

--- a/solution.py
+++ b/solution.py
@@ -351,7 +351,7 @@
     def two_copy(unit, way):
         span = pl.ds(0, len(units[unit]) * rows + 8)
         return remote(
-            two_out.at[unit, way, span], two_in.at[unit, way, span], two_send.at[unit], two_recv.at[unit],
+            two_out.at[unit, way, span], two_in.at[unit, way, span], two_send, two_recv.at[unit],
             at(0, 0, ways[way]),
         )
 
@@ -410,7 +410,7 @@
     def finish(unit):
         count = len(units[unit])
         ref = two_in.at[unit, :, pl.ds(0, count * rows + 8)]
-        remote(ref, ref, two_send.at[unit], two_recv.at[unit], sibling).wait_recv()
+        remote(ref, ref, two_send, two_recv.at[unit], sibling).wait_recv()
         incoming = [(two_in, 0), (two_in, 1)]
         if unit in direct:
             far_copy(unit).wait_recv()
@@ -487,11 +487,12 @@
     remote(ref, ref, tok_send, tok_send, sibling).wait_send()
     for unit in range(len(units)):
         for way in (0, 1):
-            two_copy(unit, way).wait_send()
             if unit not in direct:
                 one_copy(unit, way).wait_send()
         if unit in direct:
             far_copy(unit).wait_send()
+    ref = hidden.at[pl.ds(0, 5), pl.ds(0, 424)]
+    remote(ref, ref, two_send, two_send, sibling).wait_send()
     ups.drain()
     downs.drain()
 
@@ -528,7 +529,7 @@
                 vm((UNITS, 2, 2 * rows + 8, LANES), low),
                 vm((UNITS, 2, 2 * rows + 8, LANES), low),
                 dma((4,)), dma, dma((3,)),
-                dma((2, 13)), dma((2, 9)), dma((2,)), dma((2,)), dma((UNITS,)), dma((UNITS,)), dma((UNITS,)), dma((UNITS,)),
+                dma((2, 13)), dma((2, 9)), dma((2,)), dma((2,)), dma((UNITS,)), dma((UNITS,)), dma, dma((UNITS,)),
             ],
             compiler_params=pltpu.CompilerParams(
                 collective_id=0, has_side_effects=True, vmem_limit_bytes=VMEM_LIMIT

time: 63.5 us -> 63.4 us (level)
  no operation moved by 1% of the time
where the time goes in v9:
time: 63.4 us; the launch traced here: 63.3 us
  Pallas kernels  62.5 us (99%)
  local copies, waits for them, and re-layouts  0.8 us (1%)
    pallas_call x1, Pallas kernels, whole(): pl.pallas_call(kernel, out_shape=jax.ShapeDtypeStruct((rows, depth), low)...  62.5 us

profile of v9, /device:TPU:1, one launch (start us, length us, event | category | flops | bytes accessed | tf_op | source)
XLA Modules:
  0.0 63.3 jit_solution(2086670132658847637)
XLA Ops:
  0.0 62.5 %shard_map.46 = bf16[128,2048]{1,0:T(8,128)(2,1)S(1)} custom-call(bf16[128,2048]{1,0:T(8,128)(2,1)} %tok_hbm.1, f32[1,2048]{1,0:T(1,128)} %bitcast.1, f32[128,1024]{1,0:T(8,128)} %up_hbm.1, f32[1024,128]{1,0:T(8,128)} %down_hbm.1), custom_call_target="tpu_custom_call" | custom-call | tf_op jit(solution)/shard_map/pallas_call | solution.py:512
  62.5 0.8 %copy.6 = bf16[128,2048]{1,0:T(8,128)(2,1)} copy(bf16[128,2048]{1,0:T(8,128)(2,1)S(1)} %shard_map.46) | data formatting | bytes 1048576
